TPU v7x, 512 devices: a whole 4x4x16 slice. The times are simulated.
512 devices in a mesh: sp: 16 (over z), fs: 4 (over y), tp: 8 (over x, core).
Axes of the slice: x: 4, y: 4, z: 16, core: 2. Of those that a mesh axis runs over, the one named last changes fastest.
Arguments:
- tokens: bfloat16 [24576, 2048], P(('fs', 'sp', 'tp')), parts along dimension 0, may hold values from -6 to 6
- norm_gain: float32 [2048], replicated, may hold values from 0.1 to 1.9
- w_input: bfloat16 [2048, 1024], P(None, 'tp'), may hold values from -0.125 to 0.125
- w_query: bfloat16 [2048, 1024], P(None, 'tp'), may hold values from -0.125 to 0.125
- w_key: bfloat16 [2048, 1024], P(None, 'tp'), may hold values from -0.125 to 0.125
- w_value: bfloat16 [2048, 1024], P(None, 'tp'), may hold values from -0.125 to 0.125
- query_gain: float32 [64], replicated, may hold values from 0.1 to 1.9
- key_gain: float32 [64], replicated, may hold values from 0.1 to 1.9
- key_bias: bfloat16 [24576, 16], P(('fs', 'sp'), 'tp'), parts along dimension 0, may hold values from -16 to 0
- eigen_real: float32 [64, 64], P('tp'), may hold values from -32 to 0
- eigen_imag: float32 [64, 64], P('tp'), may hold values from 0.31 to 201.0624
- log_step: float32 [64], P('tp'), may hold values from -6.91 to -2.3
- input_real: float32 [64, 64, 16], P('tp'), may hold values from -1 to 1
- input_imag: float32 [64, 64, 16], P('tp'), may hold values from -1 to 1
- read_real: float32 [64, 16, 64], P('tp'), may hold values from -0.75 to 0.75
- read_imag: float32 [64, 16, 64], P('tp'), may hold values from -0.75 to 0.75
- skip_gain: float32 [1024], P('tp'), may hold values from -6 to 6
- w_out_state: bfloat16 [1024, 2048], P('tp'), may hold values from -0.125 to 0.125
- w_out_attn: bfloat16 [1024, 2048], P('tp'), may hold values from -0.125 to 0.125
Outputs:
- layer_out: bfloat16 [24576, 2048], P(('fs', 'sp', 'tp')), parts along dimension 0
There are 4 independent parts, one for each index of `fs`. A program takes and returns all parts, laid end to end along the dimension named above; an argument that names none is the same for every part. Nothing has to cross between parts.
All inputs are finite; a program needn't handle non-finite values.
Results may differ from a plain program's by a relative error of at most 0.014.
Values may be sent and summed in bfloat16 or wider, within the bound.
No kernel may reach another device: no remote copies, remote signals or barrier semaphores. Data moves between devices by JAX's collectives and lax.ppermute only.
A program may use at most 64 MiB of HBM per device.

v0:
```python
import jax
import jax.numpy as jnp
from jax import lax
from jax.experimental import pallas as pl
from jax.experimental.pallas import tpu as pltpu
from jax.sharding import Mesh
from jax.sharding import PartitionSpec as P


GROUP = 16
STATE = 64
HEAD_DIM = 64
TP = ("tp_0", "tp_1")
FS_SP_TP = ("fs", "sp", "tp_0", "tp_1")
EPSILON = 1e-06
F32 = jnp.float32
BF16 = jnp.bfloat16


MERGE_LIMIT = 16

VMEM = pl.BlockSpec(memory_space=pltpu.VMEM)
SMEM = pl.BlockSpec(memory_space=pltpu.SMEM)


def discretize(eigen_real, eigen_imag, log_step, input_real, input_imag):
    step_size = jnp.exp(log_step)[:, None]
    rotation = eigen_imag * step_size
    shrink = jnp.expm1(eigen_real * step_size)
    cosine = jnp.cos(rotation)
    sine_part = jnp.sin(rotation)
    decay_r = (1.0 + shrink) * cosine
    decay_i = (1.0 + shrink) * sine_part
    minus_r = shrink * cosine - 2.0 * jnp.square(jnp.sin(0.5 * rotation))
    modulus = jnp.square(eigen_real) + jnp.square(eigen_imag)
    factor_r = (minus_r * eigen_real + decay_i * eigen_imag) / modulus
    factor_i = (decay_i * eigen_real - minus_r * eigen_imag) / modulus
    drive_r = factor_r[..., None] * input_real - factor_i[..., None] * input_imag
    drive_i = factor_r[..., None] * input_imag + factor_i[..., None] * input_real
    return (decay_r, decay_i, drive_r, drive_i)


def split(value):
    high = value.astype(BF16)
    low = (value - high.astype(F32)).astype(BF16)
    return high, low


def cmul(ar, ai, br, bi):
    return ar * br - ai * bi, ar * bi + ai * br


def nt_dot(a, b):
    return lax.dot_general(a, b, (((1,), (1,)), ((), ())), preferred_element_type=F32)


def nn_dot(a, b):
    return jnp.dot(a, b, preferred_element_type=F32)


def lanes_low(shape):
    return lax.broadcasted_iota(jnp.int32, shape, len(shape) - 1) < HEAD_DIM


def reorder_matrix(rows, chunks, inverse):
    length = rows // chunks
    r = lax.broadcasted_iota(jnp.int32, (rows, rows), 1 if inverse else 0)
    t = lax.broadcasted_iota(jnp.int32, (rows, rows), 0 if inverse else 1)
    source = (r & (chunks - 1)) * length + (r >> 3)
    return jnp.where(t == source, 1.0, 0.0).astype(BF16)


def norm_kernel(tokens_ref, gain_ref, out_ref):
    wide = tokens_ref[...].astype(F32)
    mean = jnp.sum(wide * wide, axis=1, keepdims=True) * (1.0 / wide.shape[1])
    normed = (wide * lax.rsqrt(mean + EPSILON) * gain_ref[...]).astype(BF16)
    for k in range(out_ref.shape[0]):
        out_ref[k] = normed


def half_project_kernel(mine_ref, w_ref, found_ref):
    found_ref[...] = nn_dot(mine_ref[...], w_ref[...]).astype(BF16)


def merge_kernel(place_ref, parts_ref, mine_ref, other_ref, out_ref):
    core = place_ref[1]
    total = None
    for a in range(mine_ref.shape[0]):
        for ref, where in ((mine_ref, core), (other_ref, 1 - core)):
            term = nn_dot(parts_ref[2 * a + where], ref[a])
            total = term if total is None else total + term
    out_ref[...] = total.astype(BF16)


def block_diagonal(parts, channels, width):
    row = lax.broadcasted_iota(jnp.int32, (channels, width), 0) >> 4
    lane = lax.broadcasted_iota(jnp.int32, (channels, width), 1) >> 6
    return split(jnp.concatenate([jnp.where(row == lane, p, 0.0) for p in parts], axis=1))


def drive_matrices(lines_ref, channels):
    width = lines_ref.shape[1]
    parts = [lines_ref[j * GROUP : (j + 1) * GROUP, :] for j in range(2)]
    parts = [jnp.concatenate([p] * (channels // GROUP), axis=0) for p in parts]
    return block_diagonal(parts, channels, width)


def read_matrices(reads_ref, width):
    channels = reads_ref.shape[0] // 2
    parts = [reads_ref[j * channels : (j + 1) * channels, :] for j in range(2)]
    parts = [jnp.concatenate([p] * (width // 128), axis=1) for p in (parts[0], -parts[1])]
    return block_diagonal(parts, channels, width)


def prepare_kernel(decay_ref, tab_ref, chunk_ref, wide_ref, later_ref, *, blocks, chunk):
    rows = later_ref.shape
    below = lax.broadcasted_iota(jnp.int32, rows, 0) > lax.broadcasted_iota(jnp.int32, rows, 1)
    later_ref[...] = jnp.where(below, 1.0, 0.0).astype(BF16)
    dr, di = decay_ref[0:1, :], decay_ref[1:2, :]
    width = dr.shape[1]
    half = width // 2
    squares = [(dr, di)]
    for _ in range(9):
        a, b = squares[-1]
        squares.append(cmul(a, b, a, b))

    def power(n):
        out = None
        for k in range(10):
            if n >> k & 1:
                out = squares[k] if out is None else cmul(*out, *squares[k])
        return out

    p_chunk = power(chunk)
    p_block = power(chunk * 8)
    now = (jnp.ones_like(dr), jnp.zeros_like(dr))
    for k in range(blocks):
        for j, part in enumerate(now):
            tab_ref[4 * k + 2 * j : 4 * k + 2 * j + 1, :] = part[:, :half]
            tab_ref[4 * k + 2 * j + 1 : 4 * k + 2 * j + 2, :] = part[:, half:]
        now = cmul(*now, *p_block)
    now = (dr, di)
    for c in range(8):
        chunk_ref[c : c + 1, :width] = now[0]
        chunk_ref[c : c + 1, width:] = now[1]
        now = cmul(*now, *p_chunk)
    p2 = cmul(*p_chunk, *p_chunk)
    p4 = cmul(*p2, *p2)
    for k, (a, b) in enumerate([(dr, di), p_chunk, p2, p4]):
        wide_ref[k : k + 1, :width] = a
        wide_ref[k : k + 1, width:] = b
    wide_ref[4:8, :] = jnp.zeros((4, 2 * width), F32)


def make_push(u_perm, b_hi, b_lo, push_ref):
    push_ref[...] = nn_dot(u_perm, b_hi) + nn_dot(u_perm, b_lo)


def project_kernel(
    place_ref, found_ref, other_ref, w_ref, qg_ref, kg_ref, bias_ref, lines_ref, wide_ref,
    q_ref, payload_ref, u_ref, init_ref, rows_ref, push_ref,
):
    rows = payload_ref.shape[0] - 16
    piece = rows // 8
    core = place_ref[1]
    found_other = nn_dot(other_ref[...], w_ref[...]).astype(BF16)
    for found, where in ((found_ref[...], core), (found_other, 1 - core)):
        for a in range(4):
            at = pl.multiple_of((2 * a + where) * piece, 16)
            rows_ref[pl.ds(at, piece), :] = found[a * piece : (a + 1) * piece, :]
    low = lanes_low((rows, 2 * HEAD_DIM))

    def normed(raw, gain):
        wide = raw.astype(F32)
        square = wide * wide
        first = jnp.sum(jnp.where(low, square, 0.0), axis=1, keepdims=True)
        second = jnp.sum(jnp.where(low, 0.0, square), axis=1, keepdims=True)
        scale = jnp.where(
            low,
            lax.rsqrt(first * (1.0 / HEAD_DIM) + EPSILON),
            lax.rsqrt(second * (1.0 / HEAD_DIM) + EPSILON),
        )
        return (wide * scale * gain).astype(BF16)

    u = rows_ref[:, 0:128]
    u_perm = nn_dot(reorder_matrix(rows, 8, False), u).astype(BF16)
    u_ref[...] = u_perm
    make_push(u_perm, *drive_matrices(lines_ref, u_perm.shape[1]), push_ref)
    queries = normed(rows_ref[:, 128:256], qg_ref[...]).astype(F32) * HEAD_DIM ** (-0.5)
    q_ref[0] = jnp.where(low, queries, 0.0).astype(BF16)
    q_ref[1] = jnp.where(low, 0.0, queries).astype(BF16)
    payload_ref[0:rows, 0:128] = normed(rows_ref[:, 256:384], kg_ref[...])
    payload_ref[0:rows, 128:256] = rows_ref[:, 384:512]
    width = push_ref.shape[1] // 2
    lr = jnp.broadcast_to(wide_ref[0:1, :width], (8, width))
    li = jnp.broadcast_to(wide_ref[0:1, width:], (8, width))

    def step(k, carried):
        sr, si = carried
        at = pl.multiple_of(k * 8, 8)
        nr = lr * sr - li * si + push_ref[pl.ds(at, 8), :width]
        ni = lr * si + li * sr + push_ref[pl.ds(at, 8), width:]
        return nr, ni

    zero = jnp.zeros((8, width), F32)
    er, ei = lax.fori_loop(0, piece, step, (zero, zero), unroll=8)
    place = lax.broadcasted_iota(jnp.int32, (8, width), 0)
    for k in range(3):
        shift = 1 << k
        pr, pi = wide_ref[k + 1 : k + 2, :width], wide_ref[k + 1 : k + 2, width:]
        br = jnp.where(place >= shift, pltpu.roll(er, shift, 0), 0.0)
        bi = jnp.where(place >= shift, pltpu.roll(ei, shift, 0), 0.0)
        er, ei = er + pr * br - pi * bi, ei + pr * bi + pi * br
    init_ref[:, :width] = jnp.where(place >= 1, pltpu.roll(er, 1, 0), 0.0)
    init_ref[:, width:] = jnp.where(place >= 1, pltpu.roll(ei, 1, 0), 0.0)
    half = width // 2
    end = [er[7:8, :half], er[7:8, half:], ei[7:8, :half], ei[7:8, half:]]
    highs = [e.astype(BF16).astype(F32) for e in end]
    lows = [e - h for e, h in zip(end, highs)]
    tail = jnp.concatenate([bias_ref[...].astype(F32)] + highs + lows, axis=0)
    payload_ref[rows : rows + 16, :] = tail.astype(BF16)


def read_states(states_ref, ct_hi, ct_lo):
    high, low = split(states_ref[...])
    return nt_dot(high, ct_hi) + nt_dot(low, ct_hi) + nt_dot(high, ct_lo)


def local_state_kernel(
    u_ref, init_ref, lines_ref, wide_ref, reads_ref, skip_ref, y_ref, push_ref
):
    make_push(u_ref[...], *drive_matrices(lines_ref, u_ref.shape[1]), push_ref)
    width = push_ref.shape[1] // 2
    lr = jnp.broadcast_to(wide_ref[0:1, :width], (8, width))
    li = jnp.broadcast_to(wide_ref[0:1, width:], (8, width))

    def step(k, carried):
        sr, si = carried
        at = pl.multiple_of(k * 8, 8)
        nr = lr * sr - li * si + push_ref[pl.ds(at, 8), :width]
        ni = lr * si + li * sr + push_ref[pl.ds(at, 8), width:]
        push_ref[pl.ds(at, 8), :width] = nr
        push_ref[pl.ds(at, 8), width:] = ni
        return nr, ni

    lax.fori_loop(
        0, push_ref.shape[0] // 8, step, (init_ref[:, :width], init_ref[:, width:]), unroll=8
    )
    y_ref[...] = (
        read_states(push_ref, *read_matrices(reads_ref, width))
        + skip_ref[...] * u_ref[...].astype(F32)
    )


def score_block(q_ref, payload_ref, later_ref, diagonal):
    rows = q_ref.shape[1]
    keys, values = payload_ref[0:rows, 0:128], payload_ref[0:rows, 128:256]
    tail = payload_ref[rows : rows + 16, :].astype(F32)
    biases = (
        jnp.concatenate([tail[0:1, :], tail[1:2, 0:128]], axis=1),
        jnp.concatenate([tail[1:2, 128:256], tail[2:3, :]], axis=1),
    )
    outs, totals = [], []
    for h in range(2):
        z = nt_dot(q_ref[h], keys) + biases[h]
        loss = jnp.log(1.0 + jnp.exp(z))
        if diagonal:
            causal = lax.broadcasted_iota(jnp.int32, z.shape, 1) < lax.broadcasted_iota(
                jnp.int32, z.shape, 0
            )
            masked = jnp.where(causal, loss, 0.0)
        else:
            masked = loss
        later = nn_dot(masked.astype(BF16), later_ref[...])
        weights = jnp.exp((z - loss) - later)
        if diagonal:
            weights = jnp.where(causal, weights, 0.0)
        outs.append(nn_dot(weights.astype(BF16), values))
        totals.append(later[:, 0:1] + masked[:, 0:1])
    low = lanes_low((rows, 128))
    return jnp.where(low, outs[0], outs[1]), jnp.where(low, totals[0], totals[1])


def first_kernel(q_ref, payload_ref, later_ref, *refs):
    *state_refs, acc_ref, tot_ref, y_ref, states_ref = refs
    local_state_kernel(*state_refs, y_ref, states_ref)
    out, total = score_block(q_ref, payload_ref, later_ref, True)
    acc_ref[...] = out
    tot_ref[...] = total


def entering_state(payload_ref, tab_ref, carry_ref, power):
    rows = payload_ref.shape[0] - 16
    tail = payload_ref[rows : rows + 16, :].astype(F32)
    er, ei = tail[8:10] + tail[12:14], tail[10:12] + tail[14:16]
    wr, wi = tab_ref[4 * power : 4 * power + 2, :], tab_ref[4 * power + 2 : 4 * power + 4, :]
    carry_ref[0:2, :] += wr * er - wi * ei
    carry_ref[2:4, :] += wr * ei + wi * er


def step_kernel(
    place_ref, q_ref, later_ref, tab_ref, up_ref, down_ref,
    acc_in, tot_in, wrap_in, carry_in, acc_ref, tot_ref, wrap_ref, carry_ref, *, step, blocks,
):
    here = place_ref[0]
    acc_ref[...] = acc_in[...]
    tot_ref[...] = tot_in[...]
    wrap_ref[...] = wrap_in[...]
    carry_ref[...] = carry_in[...]
    if step < blocks // 2:

        @pl.when(here >= step)
        def _():
            out, total = score_block(q_ref, up_ref, later_ref, False)
            acc_ref[...] += out * jnp.exp(-tot_ref[...])
            tot_ref[...] += total
            entering_state(up_ref, tab_ref, carry_ref, step - 1)

    @pl.when(here >= blocks - step)
    def _():
        out, total = score_block(q_ref, down_ref, later_ref, False)
        wrap_ref[...] = wrap_ref[...] * jnp.exp(-total) + out
        entering_state(down_ref, tab_ref, carry_ref, blocks - 1 - step)


def finish_kernel(
    acc_ref, tot_ref, wrap_ref, carry_ref, y_ref, chunk_ref, wide_ref, reads_ref,
    out_ref, states_ref,
):
    rows = acc_ref.shape[0]
    width = states_ref.shape[1] // 2
    sr = jnp.concatenate([carry_ref[0:1, :], carry_ref[1:2, :]], axis=1)
    si = jnp.concatenate([carry_ref[2:3, :], carry_ref[3:4, :]], axis=1)
    zr, zi = cmul(chunk_ref[:, :width], chunk_ref[:, width:], sr, si)
    lr = jnp.broadcast_to(wide_ref[0:1, :width], (8, width))
    li = jnp.broadcast_to(wide_ref[0:1, width:], (8, width))

    def step(k, carried):
        zr, zi = carried
        at = pl.multiple_of(k * 8, 8)
        states_ref[pl.ds(at, 8), :width] = zr
        states_ref[pl.ds(at, 8), width:] = zi
        return cmul(lr, li, zr, zi)

    lax.fori_loop(0, rows // 8, step, (zr, zi), unroll=8)
    mixed = y_ref[...] + read_states(states_ref, *read_matrices(reads_ref, width))
    state_out = jax.nn.gelu(mixed).astype(BF16)
    state_out = nn_dot(reorder_matrix(rows, 8, True), state_out).astype(BF16)
    attended = acc_ref[...] + wrap_ref[...] * jnp.exp(-tot_ref[...])
    low = lanes_low(attended.shape)
    square = attended * attended
    first = jnp.sum(jnp.where(low, square, 0.0), axis=1, keepdims=True)
    second = jnp.sum(jnp.where(low, 0.0, square), axis=1, keepdims=True)
    scale = jnp.where(
        low,
        lax.rsqrt(first * (1.0 / HEAD_DIM) + EPSILON),
        lax.rsqrt(second * (1.0 / HEAD_DIM) + EPSILON),
    )
    attn_out = (attended * scale).astype(BF16)
    out_ref[:, 0:128] = state_out
    out_ref[:, 128:256] = attn_out


def call(kernel, outs, args, scratch=(), smem=0, flops=1, aliases={}, limit=16):
    return pl.pallas_call(
        kernel,
        out_shape=outs,
        in_specs=[SMEM] * smem + [VMEM] * (len(args) - smem),
        out_specs=jax.tree.map(lambda _: VMEM, outs),
        scratch_shapes=list(scratch),
        input_output_aliases=aliases,
        compiler_params=pltpu.CompilerParams(vmem_limit_bytes=limit * 2**20),
        cost_estimate=pl.CostEstimate(flops=flops, bytes_accessed=10**6, transcendentals=0),
    )(*args)


def shape(dims, dtype=F32):
    return jax.ShapeDtypeStruct(dims, dtype)


def on_device(
    tokens,
    norm_gain,
    w_input,
    w_query,
    w_key,
    w_value,
    query_gain,
    key_gain,
    key_bias,
    eigen_real,
    eigen_imag,
    log_step,
    input_real,
    input_imag,
    read_real,
    read_imag,
    skip_gain,
    w_out_state,
    w_out_attn,
):
    blocks = lax.axis_size("sp")
    rows = key_bias.shape[0]
    piece = rows // 8
    groups = eigen_real.shape[0]
    width = groups * STATE
    channels = groups * GROUP
    place = jnp.stack([lax.axis_index("sp"), lax.axis_index("tp_1")]).astype(jnp.int32)

    copies = call(
        norm_kernel,
        shape((4, *tokens.shape), BF16),
        (tokens, norm_gain.reshape(1, -1)),
    )
    mine = lax.all_to_all(copies, "tp_0", 0, 0, tiled=True).reshape(4 * piece, -1)

    w_joined = jnp.concatenate([w_input, w_query, w_key, w_value], axis=1)
    w_out = jnp.concatenate([w_out_state, w_out_attn], axis=0)
    w_out_copies = jnp.broadcast_to(w_out[None], (4, *w_out.shape))
    decay_r, decay_i, drive_r, drive_i = discretize(
        eigen_real, eigen_imag, log_step, input_real, input_imag
    )
    lines = jnp.concatenate(
        [jnp.transpose(part, (2, 0, 1)).reshape(GROUP, width) for part in (drive_r, drive_i)]
    )
    reads = [part.reshape(channels, STATE) for part in (read_real, read_imag)]
    reads = jnp.concatenate([jnp.concatenate([part, part], axis=1) for part in reads])
    decay = jnp.stack([decay_r.reshape(-1), decay_i.reshape(-1)])
    bias8 = jnp.pad(jnp.transpose(key_bias).reshape(-1, 256), ((0, 5), (0, 0)))
    gains = [jnp.tile(g, 2).reshape(1, 128) for g in (query_gain, key_gain)]
    skip = skip_gain.reshape(1, -1)
    decay, lines, reads, w_joined, w_out_copies, bias8, gains, skip, place = (
        lax.optimization_barrier(
            (decay, lines, reads, w_joined, w_out_copies, bias8, gains, skip, place)
        )
    )
    tables = call(
        lambda *refs: prepare_kernel(*refs, blocks=blocks, chunk=piece),
        (
            shape((4 * blocks, width // 2)),
            shape((8, 2 * width)),
            shape((8, 2 * width)),
            shape((rows, rows), BF16),
        ),
        (decay,),
    )
    mine, tables = lax.optimization_barrier((mine, tables))
    tab, chunk, wide, later = tables
    other = lax.ppermute(mine, "tp_1", [(0, 1), (1, 0)])

    found = call(
        half_project_kernel, shape((4 * piece, 512), BF16), (mine, w_joined), flops=10**9
    )
    q, payload, u_perm, init = call(
        project_kernel,
        (
            shape((2, rows, 128), BF16),
            shape((rows + 16, 256), BF16),
            shape((rows, channels), BF16),
            shape((8, 2 * width)),
        ),
        (place, found, other, w_joined, *gains, bias8, lines, wide),
        scratch=(pltpu.VMEM((rows, 512), BF16), pltpu.VMEM((rows, 2 * width), F32)),
        smem=1,
        flops=4 * 10**9,
    )

    acc, tot, y_local = call(
        first_kernel,
        (shape((rows, 128)), shape((rows, 128)), shape((rows, channels))),
        (q, payload, later, u_perm, init, lines, wide, reads, skip),
        scratch=(pltpu.VMEM((rows, 2 * width), F32),),
        flops=4 * 10**9,
    )
    wrap = jnp.zeros((rows, 128), F32)
    carry = jnp.zeros((8, width // 2), F32)
    up = down = payload
    half = blocks // 2
    for step in range(1, half + 1):
        if step < half:
            up = lax.ppermute(up, "sp", [(i - 1, i) for i in range(step, blocks)])
        down = lax.ppermute(
            down, "sp", [((j - step + 1) % blocks, (j - step) % blocks) for j in range(half)]
        )
        acc, tot, wrap, carry = call(
            lambda *refs, step=step: step_kernel(*refs, step=step, blocks=blocks),
            (shape((rows, 128)), shape((rows, 128)), shape((rows, 128)), shape(carry.shape)),
            (place, q, later, tab, up, down, acc, tot, wrap, carry),
            smem=1,
            flops=3 * 10**9,
            aliases={6: 0, 7: 1, 8: 2, 9: 3},
        )
        if step == 1:
            acc, w_out_copies = lax.optimization_barrier((acc, w_out_copies))
            w_out_mine = lax.all_to_all(w_out_copies, "tp_0", 0, 0, tiled=True)
        if step == half - 1:
            acc, w_out_mine = lax.optimization_barrier((acc, w_out_mine))
            w_out_other = lax.ppermute(w_out_mine, "tp_1", [(0, 1), (1, 0)])
    both = call(
        finish_kernel,
        shape((rows, 2 * channels), BF16),
        (acc, tot, wrap, carry, y_local, chunk, wide, reads),
        scratch=(pltpu.VMEM((rows, 2 * width), F32),),
        flops=3 * 10**9,
    )
    parts = lax.all_to_all(both.reshape(8, piece, -1), TP, 0, 0, tiled=True)
    return call(
        merge_kernel,
        shape((piece, w_out.shape[1]), BF16),
        (place, parts, w_out_mine, w_out_other),
        smem=1,
        flops=10**9,
        limit=MERGE_LIMIT,
    )


def solution(mesh):
    torus = Mesh(
        mesh.devices.reshape(mesh.shape["sp"], mesh.shape["fs"], 4, 2), ("sp", "fs", "tp_0", "tp_1")
    )
    placed = (
        P(FS_SP_TP, None),
        P(),
        P(None, TP),
        P(None, TP),
        P(None, TP),
        P(None, TP),
        P(),
        P(),
        P(("fs", "sp"), TP),
        P(TP, None),
        P(TP, None),
        P(TP),
        P(TP, None, None),
        P(TP, None, None),
        P(TP, None, None),
        P(TP, None, None),
        P(TP),
        P(TP, None),
        P(TP, None),
    )

    return jax.shard_map(
        on_device, mesh=torus, in_specs=placed, out_specs=P(FS_SP_TP, None), check_vma=False
    )
```

profile of v0, /device:TPU:1, one launch (start us, length us, event | category | flops | bytes accessed | tf_op | source)
XLA Modules:
  0.0 139.1 jit_solution(11721637243202621559)
XLA Ops:
  0.0 0.9 copy-done
  0.9 0.7 copy-done.1
  1.6 1.1 shard_map.181
  2.7 4.8 %all-to-all-start = ((bf16[4,48,2048]{2,1,0:T(8,128)(2,1)}), bf16[4,48,2048]{2,1,0:T(8,128)(2,1)S(1)}, u32[]{:S(2)}, u32[]{:S(2)}) async-start(bf16[4,48,2048]{2,1,0:T(8,128)(2,1)} %shard_map.181), calls=%async_computation | async-start | bytes 1572864 | tf_op jit(solution)/shard_map/all_to_all | solution.py:415
  7.5 0.7 exp.3
  8.2 0.7 tile.4
  8.8 0.1 reshape_tile.6.qg_ref
  8.9 0.7 tile.5
  9.6 0.1 reshape_tile.7.kg_ref
  9.7 0.7 reshape.37
  10.4 0.8 fusion
  11.2 0.1 stack_reshape.7
  11.3 0.1 stack_reshape.6
  11.3 0.9 subtract_bitcast_fusion
  12.3 0.1 reshape.33
  12.4 0.1 reshape.34
  12.5 1.0 maximum_maximum_fusion.refs_4_.reads_ref
  13.5 0.1 pad_add_fusion.place_ref.refs_0_
  13.6 1.3 pad_maximum_fusion.1
  14.9 1.7 %pad_maximum_fusion.w_ref = bf16[2048,512]{1,0:T(8,128)(2,1)S(1)} fusion(bf16[2048,128]{1,0:T(8,128)(2,1)} %param.24, bf16[2048,128]{1,0:T(8,128)(2,1)} %param.23, bf16[2048,128]{1,0:T(8,128)(2,1)} %param.22, bf16[2048,128]{1,0:T(8,128)(2,1)} %param.21), kind=kLoop, calls=%fused_computation | loop fusion | flops 8388608 | bytes 4194304 | tf_op jit(solution)/shard_map/concatenate | solution.py:417
  16.7 2.5 %broadcast_in_dim.6 = bf16[4,256,2048]{2,1,0:T(8,128)(2,1)} broadcast(bf16[256,2048]{1,0:T(8,128)(2,1)S(1)} %pad_maximum_fusion.1), dimensions={1,2} | broadcast | bytes 5242880 | tf_op jit(solution)/shard_map/broadcast_in_dim | solution.py:419
  19.1 0.1 shard_map.182
  19.2 7.4 %collective-permute-start = (bf16[192,2048]{1,0:T(8,128)(2,1)S(1)}, bf16[192,2048]{1,0:T(8,128)(2,1)S(1)}, u32[]{:S(2)}, u32[]{:S(2)}) collective-permute-start(bf16[192,2048]{1,0:T(8,128)(2,1)S(1)} %bitcast.13), channel_id=1, source_target_pairs={{0,1},{1,0},{2,3},{3,2},{4,5},{5,4},{6,7},{7,6},{8,9},{9,8},{10,11... | collective-permute-start | bytes 2359304 | tf_op jit(solution)/shard_map/ppermute | solution.py:449
  26.7 0.6 shard_map.183.found_ref
  27.3 1.3 collective-permute-done.other_ref
  28.6 2.3 %shard_map.184 = (bf16[2,384,128]{2,1,0:T(8,128)(2,1)S(1)}, bf16[400,256]{1,0:T(8,128)(2,1)S(1)}, bf16[384,128]{1,0:T(8,128)(2,1)S(1)}, f32[8,1024]{1,0:T(8,128)S(1)}) custom-call(s32[2]{0:T(128)S(1)} %pad_add_fusion.place_ref.refs_0_, bf16[192,512]{1,0:T(8,128)(2,1)S(1)} %shard_map.183.found_ref, bf16[192,2048]{1,0:T(8,128)(2,1)S(1)} %collective-permute-done.other_ref, ...), custom_call_target="tpu_custom_call" | custom-call | flops 4000000000 | bytes 1000000 | tf_op jit(solution)/shard_map/pallas_call | solution.py:365
  30.8 7.1 %collective-permute-start.8 = (bf16[400,256]{1,0:T(8,128)(2,1)S(1)}, bf16[400,256]{1,0:T(8,128)(2,1)S(1)}, u32[]{:S(2)}, u32[]{:S(2)}) collective-permute-start(bf16[400,256]{1,0:T(8,128)(2,1)S(1)} %get-tuple-element.83.payload_ref), channel_id=1, source_target_pairs={{0,480},{32,0},{64,32},{96,64},{128,96},{160,128},{192,160},{224,1... | collective-permute-start | bytes 614408 | tf_op jit(solution)/shard_map/ppermute | solution.py:482
  38.0 1.3 collective-permute-start.1
  39.3 2.7 %shard_map.185 = (f32[384,128]{1,0:T(8,128)S(1)}, f32[384,128]{1,0:T(8,128)S(1)}, f32[384,128]{1,0:T(8,128)S(1)}) custom-call(bf16[2,384,128]{2,1,0:T(8,128)(2,1)S(1)} %get-tuple-element.80.q_ref.refs_1_, bf16[400,256]{1,0:T(8,128)(2,1)S(1)} %get-tuple-element.83.payload_ref, bf16[384,384]{1,0:T(8,128)(2,1)S(1)} %get-tuple-element.81.later_ref.refs_2_, ...), custom_call_target="tpu_custom_call" | custom-call | flops 4000000000 | bytes 1000000 | tf_op jit(solution)/shard_map/pallas_call | solution.py:365
  42.0 0.0 collective-permute-done.8.refs_5_
  42.0 1.3 collective-permute-done.1.refs_4_
  43.3 0.6 shard_map.186
  43.9 4.9 %all-to-all-start.1 = ((bf16[4,256,2048]{2,1,0:T(8,128)(2,1)}), bf16[4,256,2048]{2,1,0:T(8,128)(2,1)}, u32[]{:S(2)}, u32[]{:S(2)}) async-start(bf16[4,256,2048]{2,1,0:T(8,128)(2,1)} %broadcast_in_dim.6), calls=%async_computation.1 | async-start | bytes 8388608 | tf_op jit(solution)/shard_map/all_to_all | solution.py:495
  48.8 6.7 %collective-permute-start.9 = (bf16[400,256]{1,0:T(8,128)(2,1)S(1)}, bf16[400,256]{1,0:T(8,128)(2,1)S(1)}, u32[]{:S(2)}, u32[]{:S(2)}) collective-permute-start(bf16[400,256]{1,0:T(8,128)(2,1)S(1)} %collective-permute-done.8.refs_5_), channel_id=1, source_target_pairs={{480,448},{0,480},{32,0},{64,32},{96,64},{128,96},{160,128},{192,1... | collective-permute-start | bytes 614408 | tf_op jit(solution)/shard_map/ppermute | solution.py:482
  55.5 0.7 collective-permute-start.2
  56.2 2.5 %collective-permute-done.9.refs_5_ = bf16[400,256]{1,0:T(8,128)(2,1)S(1)} collective-permute-done((bf16[400,256]{1,0:T(8,128)(2,1)S(1)}, bf16[400,256]{1,0:T(8,128)(2,1)S(1)}, u32[]{:S(2)}, u32[]{:S(2)}) %collective-permute-start.9) | collective-permute-done | bytes 204832 | tf_op jit(solution)/shard_map/ppermute | solution.py:482
  58.7 5.4 %collective-permute-start.10 = (bf16[400,256]{1,0:T(8,128)(2,1)S(1)}, bf16[400,256]{1,0:T(8,128)(2,1)S(1)}, u32[]{:S(2)}, u32[]{:S(2)}) collective-permute-start(bf16[400,256]{1,0:T(8,128)(2,1)S(1)} %collective-permute-done.9.refs_5_), channel_id=1, source_target_pairs={{448,416},{480,448},{0,480},{32,0},{64,32},{96,64},{128,96},{160,1... | collective-permute-start | bytes 614408 | tf_op jit(solution)/shard_map/ppermute | solution.py:482
  64.1 0.7 collective-permute-start.3
  64.8 0.6 shard_map.187
  65.4 1.4 collective-permute-done.10.refs_5_
  66.8 5.4 %collective-permute-start.11 = (bf16[400,256]{1,0:T(8,128)(2,1)S(1)}, bf16[400,256]{1,0:T(8,128)(2,1)S(1)}, u32[]{:S(2)}, u32[]{:S(2)}) collective-permute-start(bf16[400,256]{1,0:T(8,128)(2,1)S(1)} %collective-permute-done.10.refs_5_), channel_id=1, source_target_pairs={{416,384},{448,416},{480,448},{0,480},{32,0},{64,32},{96,64},{128,... | collective-permute-start | bytes 614408 | tf_op jit(solution)/shard_map/ppermute | solution.py:482
  72.2 0.7 collective-permute-start.4
  72.9 0.8 shard_map.188
  73.7 1.2 collective-permute-done.11.refs_5_
  74.9 5.4 %collective-permute-start.12 = (bf16[400,256]{1,0:T(8,128)(2,1)S(1)}, bf16[400,256]{1,0:T(8,128)(2,1)S(1)}, u32[]{:S(2)}, u32[]{:S(2)}) collective-permute-start(bf16[400,256]{1,0:T(8,128)(2,1)S(1)} %collective-permute-done.11.refs_5_), channel_id=1, source_target_pairs={{384,352},{416,384},{448,416},{480,448},{0,480},{32,0},{64,32},{96... | collective-permute-start | bytes 614408 | tf_op jit(solution)/shard_map/ppermute | solution.py:482
  80.3 0.7 collective-permute-start.5
  81.0 0.6 shard_map.189
  81.6 1.4 collective-permute-done.12.refs_5_
  83.0 5.4 %collective-permute-start.13 = (bf16[400,256]{1,0:T(8,128)(2,1)S(1)}, bf16[400,256]{1,0:T(8,128)(2,1)S(1)}, u32[]{:S(2)}, u32[]{:S(2)}) collective-permute-start(bf16[400,256]{1,0:T(8,128)(2,1)S(1)} %collective-permute-done.12.refs_5_), channel_id=1, source_target_pairs={{352,320},{384,352},{416,384},{448,416},{480,448},{0,480},{32,0},{... | collective-permute-start | bytes 614408 | tf_op jit(solution)/shard_map/ppermute | solution.py:482
  88.4 0.7 collective-permute-start.6
  89.1 0.6 shard_map.190
  89.7 1.4 collective-permute-done.13.refs_5_
  91.1 5.4 %collective-permute-start.14 = (bf16[400,256]{1,0:T(8,128)(2,1)S(1)}, bf16[400,256]{1,0:T(8,128)(2,1)S(1)}, u32[]{:S(2)}, u32[]{:S(2)}) collective-permute-start(bf16[400,256]{1,0:T(8,128)(2,1)S(1)} %collective-permute-done.13.refs_5_), channel_id=1, source_target_pairs={{320,288},{352,320},{384,352},{416,384},{448,416},{480,448},{0,480... | collective-permute-start | bytes 614408 | tf_op jit(solution)/shard_map/ppermute | solution.py:482
  96.5 0.7 collective-permute-start.7
  97.2 0.6 shard_map.191
  97.8 1.4 collective-permute-done.14.refs_5_
  99.2 0.6 shard_map.192
  99.8 7.8 %collective-permute-start.16 = (bf16[4,256,2048]{2,1,0:T(8,128)(2,1)}, bf16[4,256,2048]{2,1,0:T(8,128)(2,1)S(1)}, u32[]{:S(2)}, u32[]{:S(2)}) collective-permute-start(bf16[4,256,2048]{2,1,0:T(8,128)(2,1)} %all-to-all-done.1.mine_ref), channel_id=1, source_target_pairs={{0,1},{1,0},{2,3},{3,2},{4,5},{5,4},{6,7},{7,6},{8,9},{9,8},{10,11... | collective-permute-start | bytes 12582920 | tf_op jit(solution)/shard_map/ppermute | solution.py:498
  107.6 9.8 %collective-permute-start.15 = (bf16[400,256]{1,0:T(8,128)(2,1)S(1)}, bf16[400,256]{1,0:T(8,128)(2,1)S(1)}, u32[]{:S(2)}, u32[]{:S(2)}) collective-permute-start(bf16[400,256]{1,0:T(8,128)(2,1)S(1)} %collective-permute-done.14.refs_5_), channel_id=1, source_target_pairs={{288,256},{320,288},{352,320},{384,352},{416,384},{448,416},{480,4... | collective-permute-start | bytes 614408 | tf_op jit(solution)/shard_map/ppermute | solution.py:482
  117.4 4.4 %collective-permute-done.15.refs_5_ = bf16[400,256]{1,0:T(8,128)(2,1)S(1)} collective-permute-done((bf16[400,256]{1,0:T(8,128)(2,1)S(1)}, bf16[400,256]{1,0:T(8,128)(2,1)S(1)}, u32[]{:S(2)}, u32[]{:S(2)}) %collective-permute-start.15) | collective-permute-done | bytes 204832 | tf_op jit(solution)/shard_map/ppermute | solution.py:482
  121.8 0.6 shard_map.193
  122.4 1.2 shard_map.194
  123.7 11.0 %all_to_all.15.parts_ref = bf16[8,48,256]{2,1,0:T(8,128)(2,1)S(1)} all-to-all(bf16[8,48,256]{2,1,0:T(8,128)(2,1)S(1)} %bitcast.15), channel_id=1, replica_groups=mesh['sp'=16,'fs'=4,'tp_0'=4,'tp_1'=2] {'tp_0','tp_1'}, dimensions={0} | all-to-all | bytes 393216 | tf_op jit(solution)/shard_map/all_to_all | solution.py:506
  134.7 4.4 %shard_map.195 = bf16[48,2048]{1,0:T(8,128)(2,1)} custom-call(s32[2]{0:T(128)S(1)} %pad_add_fusion.place_ref.refs_0_, bf16[8,48,256]{2,1,0:T(8,128)(2,1)S(1)} %all_to_all.15.parts_ref, bf16[4,256,2048]{2,1,0:T(8,128)(2,1)} %all-to-all-done.1.mine_ref, bf16[4,256,2048]{2,1,0:T(8,128)(2,1)S(1)} %collective-permute-done.16.other_ref), custom_call_target="tpu_custom_call" | custom-call | flops 1000000000 | bytes 1000000 | tf_op jit(solution)/shard_map/pallas_call | solution.py:365
  (20 shorter events, 0.1 us)
Async XLA Ops:
  0.0 0.9 copy-start
  0.9 0.7 copy-start.1
  2.7 16.6 %all-to-all-start = ((bf16[4,48,2048]{2,1,0:T(8,128)(2,1)}), bf16[4,48,2048]{2,1,0:T(8,128)(2,1)S(1)}, u32[]{:S(2)}, u32[]{:S(2)}) async-start(bf16[4,48,2048]{2,1,0:T(8,128)(2,1)} %shard_map.181), calls=%async_computation | async-start | bytes 1572864 | tf_op jit(solution)/shard_map/all_to_all | solution.py:415
  19.2 9.3 %collective-permute-start = (bf16[192,2048]{1,0:T(8,128)(2,1)S(1)}, bf16[192,2048]{1,0:T(8,128)(2,1)S(1)}, u32[]{:S(2)}, u32[]{:S(2)}) collective-permute-start(bf16[192,2048]{1,0:T(8,128)(2,1)S(1)} %bitcast.13), channel_id=1, source_target_pairs={{0,1},{1,0},{2,3},{3,2},{4,5},{5,4},{6,7},{7,6},{8,9},{9,8},{10,11... | collective-permute-start | bytes 2359304 | tf_op jit(solution)/shard_map/ppermute | solution.py:449
  27.3 12.0 %copy-start.2 = (f32[128]{0:T(128)S(1)}, f32[128]{0:T(128)}, u32[]{:S(2)}) copy-start(f32[128]{0:T(128)} %param.35) | copy-start | bytes 1540
  30.8 11.1 %collective-permute-start.8 = (bf16[400,256]{1,0:T(8,128)(2,1)S(1)}, bf16[400,256]{1,0:T(8,128)(2,1)S(1)}, u32[]{:S(2)}, u32[]{:S(2)}) collective-permute-start(bf16[400,256]{1,0:T(8,128)(2,1)S(1)} %get-tuple-element.83.payload_ref), channel_id=1, source_target_pairs={{0,480},{32,0},{64,32},{96,64},{128,96},{160,128},{192,160},{224,1... | collective-permute-start | bytes 614408 | tf_op jit(solution)/shard_map/ppermute | solution.py:482
  38.0 5.3 %collective-permute-start.1 = (bf16[400,256]{1,0:T(8,128)(2,1)S(1)}, bf16[400,256]{1,0:T(8,128)(2,1)S(1)}, u32[]{:S(2)}, u32[]{:S(2)}) collective-permute-start(bf16[400,256]{1,0:T(8,128)(2,1)S(1)} %get-tuple-element.83.payload_ref), channel_id=1, source_target_pairs={{0,32},{32,64},{64,96},{96,128},{128,160},{160,192},{192,224},{224... | collective-permute-start | bytes 614408 | tf_op jit(solution)/shard_map/ppermute | solution.py:481
  43.9 55.9 %all-to-all-start.1 = ((bf16[4,256,2048]{2,1,0:T(8,128)(2,1)}), bf16[4,256,2048]{2,1,0:T(8,128)(2,1)}, u32[]{:S(2)}, u32[]{:S(2)}) async-start(bf16[4,256,2048]{2,1,0:T(8,128)(2,1)} %broadcast_in_dim.6), calls=%async_computation.1 | async-start | bytes 8388608 | tf_op jit(solution)/shard_map/all_to_all | solution.py:495
  48.8 9.8 %collective-permute-start.9 = (bf16[400,256]{1,0:T(8,128)(2,1)S(1)}, bf16[400,256]{1,0:T(8,128)(2,1)S(1)}, u32[]{:S(2)}, u32[]{:S(2)}) collective-permute-start(bf16[400,256]{1,0:T(8,128)(2,1)S(1)} %collective-permute-done.8.refs_5_), channel_id=1, source_target_pairs={{480,448},{0,480},{32,0},{64,32},{96,64},{128,96},{160,128},{192,1... | collective-permute-start | bytes 614408 | tf_op jit(solution)/shard_map/ppermute | solution.py:482
  55.5 8.6 %collective-permute-start.2 = (bf16[400,256]{1,0:T(8,128)(2,1)S(1)}, bf16[400,256]{1,0:T(8,128)(2,1)S(1)}, u32[]{:S(2)}, u32[]{:S(2)}) collective-permute-start(bf16[400,256]{1,0:T(8,128)(2,1)S(1)} %collective-permute-done.1.refs_4_), channel_id=1, source_target_pairs={{32,64},{64,96},{96,128},{128,160},{160,192},{192,224},{224,256},{... | collective-permute-start | bytes 614408 | tf_op jit(solution)/shard_map/ppermute | solution.py:481
  58.7 8.1 %collective-permute-start.10 = (bf16[400,256]{1,0:T(8,128)(2,1)S(1)}, bf16[400,256]{1,0:T(8,128)(2,1)S(1)}, u32[]{:S(2)}, u32[]{:S(2)}) collective-permute-start(bf16[400,256]{1,0:T(8,128)(2,1)S(1)} %collective-permute-done.9.refs_5_), channel_id=1, source_target_pairs={{448,416},{480,448},{0,480},{32,0},{64,32},{96,64},{128,96},{160,1... | collective-permute-start | bytes 614408 | tf_op jit(solution)/shard_map/ppermute | solution.py:482
  64.1 8.1 %collective-permute-start.3 = (bf16[400,256]{1,0:T(8,128)(2,1)S(1)}, bf16[400,256]{1,0:T(8,128)(2,1)S(1)}, u32[]{:S(2)}, u32[]{:S(2)}) collective-permute-start(bf16[400,256]{1,0:T(8,128)(2,1)S(1)} %collective-permute-done.2.refs_4_), channel_id=1, source_target_pairs={{64,96},{96,128},{128,160},{160,192},{192,224},{224,256},{256,288}... | collective-permute-start | bytes 614408 | tf_op jit(solution)/shard_map/ppermute | solution.py:481
  66.8 8.1 %collective-permute-start.11 = (bf16[400,256]{1,0:T(8,128)(2,1)S(1)}, bf16[400,256]{1,0:T(8,128)(2,1)S(1)}, u32[]{:S(2)}, u32[]{:S(2)}) collective-permute-start(bf16[400,256]{1,0:T(8,128)(2,1)S(1)} %collective-permute-done.10.refs_5_), channel_id=1, source_target_pairs={{416,384},{448,416},{480,448},{0,480},{32,0},{64,32},{96,64},{128,... | collective-permute-start | bytes 614408 | tf_op jit(solution)/shard_map/ppermute | solution.py:482
  72.2 8.1 %collective-permute-start.4 = (bf16[400,256]{1,0:T(8,128)(2,1)S(1)}, bf16[400,256]{1,0:T(8,128)(2,1)S(1)}, u32[]{:S(2)}, u32[]{:S(2)}) collective-permute-start(bf16[400,256]{1,0:T(8,128)(2,1)S(1)} %collective-permute-done.3.refs_4_), channel_id=1, source_target_pairs={{96,128},{128,160},{160,192},{192,224},{224,256},{256,288},{288,32... | collective-permute-start | bytes 614408 | tf_op jit(solution)/shard_map/ppermute | solution.py:481
  74.9 8.1 %collective-permute-start.12 = (bf16[400,256]{1,0:T(8,128)(2,1)S(1)}, bf16[400,256]{1,0:T(8,128)(2,1)S(1)}, u32[]{:S(2)}, u32[]{:S(2)}) collective-permute-start(bf16[400,256]{1,0:T(8,128)(2,1)S(1)} %collective-permute-done.11.refs_5_), channel_id=1, source_target_pairs={{384,352},{416,384},{448,416},{480,448},{0,480},{32,0},{64,32},{96... | collective-permute-start | bytes 614408 | tf_op jit(solution)/shard_map/ppermute | solution.py:482
  80.3 8.1 %collective-permute-start.5 = (bf16[400,256]{1,0:T(8,128)(2,1)S(1)}, bf16[400,256]{1,0:T(8,128)(2,1)S(1)}, u32[]{:S(2)}, u32[]{:S(2)}) collective-permute-start(bf16[400,256]{1,0:T(8,128)(2,1)S(1)} %collective-permute-done.4.refs_4_), channel_id=1, source_target_pairs={{128,160},{160,192},{192,224},{224,256},{256,288},{288,320},{320,3... | collective-permute-start | bytes 614408 | tf_op jit(solution)/shard_map/ppermute | solution.py:481
  83.0 8.1 %collective-permute-start.13 = (bf16[400,256]{1,0:T(8,128)(2,1)S(1)}, bf16[400,256]{1,0:T(8,128)(2,1)S(1)}, u32[]{:S(2)}, u32[]{:S(2)}) collective-permute-start(bf16[400,256]{1,0:T(8,128)(2,1)S(1)} %collective-permute-done.12.refs_5_), channel_id=1, source_target_pairs={{352,320},{384,352},{416,384},{448,416},{480,448},{0,480},{32,0},{... | collective-permute-start | bytes 614408 | tf_op jit(solution)/shard_map/ppermute | solution.py:482
  88.4 8.1 %collective-permute-start.6 = (bf16[400,256]{1,0:T(8,128)(2,1)S(1)}, bf16[400,256]{1,0:T(8,128)(2,1)S(1)}, u32[]{:S(2)}, u32[]{:S(2)}) collective-permute-start(bf16[400,256]{1,0:T(8,128)(2,1)S(1)} %collective-permute-done.5.refs_4_), channel_id=1, source_target_pairs={{160,192},{192,224},{224,256},{256,288},{288,320},{320,352},{352,3... | collective-permute-start | bytes 614408 | tf_op jit(solution)/shard_map/ppermute | solution.py:481
  91.1 8.1 %collective-permute-start.14 = (bf16[400,256]{1,0:T(8,128)(2,1)S(1)}, bf16[400,256]{1,0:T(8,128)(2,1)S(1)}, u32[]{:S(2)}, u32[]{:S(2)}) collective-permute-start(bf16[400,256]{1,0:T(8,128)(2,1)S(1)} %collective-permute-done.13.refs_5_), channel_id=1, source_target_pairs={{320,288},{352,320},{384,352},{416,384},{448,416},{480,448},{0,480... | collective-permute-start | bytes 614408 | tf_op jit(solution)/shard_map/ppermute | solution.py:482
  96.5 2.7 %collective-permute-start.7 = (bf16[400,256]{1,0:T(8,128)(2,1)S(1)}, bf16[400,256]{1,0:T(8,128)(2,1)S(1)}, u32[]{:S(2)}, u32[]{:S(2)}) collective-permute-start(bf16[400,256]{1,0:T(8,128)(2,1)S(1)} %collective-permute-done.6.refs_4_), channel_id=1, source_target_pairs={{192,224},{224,256},{256,288},{288,320},{320,352},{352,384},{384,4... | collective-permute-start | bytes 614408 | tf_op jit(solution)/shard_map/ppermute | solution.py:481
  99.8 34.9 %collective-permute-start.16 = (bf16[4,256,2048]{2,1,0:T(8,128)(2,1)}, bf16[4,256,2048]{2,1,0:T(8,128)(2,1)S(1)}, u32[]{:S(2)}, u32[]{:S(2)}) collective-permute-start(bf16[4,256,2048]{2,1,0:T(8,128)(2,1)} %all-to-all-done.1.mine_ref), channel_id=1, source_target_pairs={{0,1},{1,0},{2,3},{3,2},{4,5},{5,4},{6,7},{7,6},{8,9},{9,8},{10,11... | collective-permute-start | bytes 12582920 | tf_op jit(solution)/shard_map/ppermute | solution.py:498
  107.6 14.2 %collective-permute-start.15 = (bf16[400,256]{1,0:T(8,128)(2,1)S(1)}, bf16[400,256]{1,0:T(8,128)(2,1)S(1)}, u32[]{:S(2)}, u32[]{:S(2)}) collective-permute-start(bf16[400,256]{1,0:T(8,128)(2,1)S(1)} %collective-permute-done.14.refs_5_), channel_id=1, source_target_pairs={{288,256},{320,288},{352,320},{384,352},{416,384},{448,416},{480,4... | collective-permute-start | bytes 614408 | tf_op jit(solution)/shard_map/ppermute | solution.py:482
where the time goes:
time: 140 us; the launch traced here: 139 us
  starting transfers between devices  80.9 us (58%)
  Pallas kernels  17.5 us (12%)
  waiting for transfers between devices  16.1 us (12%)
  blocking collectives  11 us (8%)
  local copies, waits for them, and re-layouts  7.34 us (5%)
  other arithmetic  5.89 us (4%)
    ppermute x8, starting transfers between devices, on_device(): lax.ppermute(down, 'sp', [((j - step + 1) % blocks, (j - step) % blocks)...  50.6 us
    pallas_call x15, Pallas kernels, call(): pl.pallas_call(kernel, out_shape=outs, in_specs=[SMEM] * smem + [VMEM] *...  17.5 us
    ppermute x8, waiting for transfers between devices, on_device(): lax.ppermute(down, 'sp', [((j - step + 1) % blocks, (j - step) % blocks)...  13.5 us
    all_to_all x1, blocking collectives, on_device(): parts = lax.all_to_all(both.reshape(8, piece, -1), TP, 0, 0, tiled=True)  11 us
    ppermute x1, starting transfers between devices, on_device(): w_out_other = lax.ppermute(w_out_mine, 'tp_1', [(0, 1), (1, 0)])  7.79 us
    ppermute x1, starting transfers between devices, on_device(): other = lax.ppermute(mine, 'tp_1', [(0, 1), (1, 0)])  7.42 us
    ppermute x7, starting transfers between devices, on_device(): up = lax.ppermute(up, 'sp', [(i - 1, i) for i in range(step, blocks)])  5.34 us
    all_to_all x1, starting transfers between devices, on_device(): w_out_mine = lax.all_to_all(w_out_copies, 'tp_0', 0, 0, tiled=True)  4.91 us
  transfers between devices with their start and end apart: 19, of which 9 were waited for; matrix products, arithmetic and copies ran while one was open for 8% of the time, Pallas kernels for 7%

commit v1 on v0

--- a/solution.py
+++ b/solution.py
@@ -16,8 +16,6 @@
 F32 = jnp.float32
 BF16 = jnp.bfloat16
 
-
-MERGE_LIMIT = 16
 
 VMEM = pl.BlockSpec(memory_space=pltpu.VMEM)
 SMEM = pl.BlockSpec(memory_space=pltpu.SMEM)
@@ -82,14 +80,21 @@
     found_ref[...] = nn_dot(mine_ref[...], w_ref[...]).astype(BF16)
 
 
-def merge_kernel(place_ref, parts_ref, mine_ref, other_ref, out_ref):
+def merge_kernel(place_ref, parts_ref, mine_ref, other_ref, out_ref, total_ref):
+    a = pl.program_id(0)
     core = place_ref[1]
-    total = None
-    for a in range(mine_ref.shape[0]):
-        for ref, where in ((mine_ref, core), (other_ref, 1 - core)):
-            term = nn_dot(parts_ref[2 * a + where], ref[a])
-            total = term if total is None else total + term
-    out_ref[...] = total.astype(BF16)
+
+    @pl.when(a == 0)
+    def _():
+        total_ref[...] = jnp.zeros_like(total_ref)
+
+    total_ref[...] += nn_dot(parts_ref[2 * a + core], mine_ref[0]) + nn_dot(
+        parts_ref[2 * a + 1 - core], other_ref[a]
+    )
+
+    @pl.when(a == pl.num_programs(0) - 1)
+    def _():
+        out_ref[...] = total_ref[...].astype(BF16)
 
 
 def block_diagonal(parts, channels, width):
@@ -300,14 +305,14 @@
 
 def step_kernel(
     place_ref, q_ref, later_ref, tab_ref, up_ref, down_ref,
-    acc_in, tot_in, wrap_in, carry_in, acc_ref, tot_ref, wrap_ref, carry_ref, *, step, blocks,
+    acc_in, tot_in, wrap_in, carry_in, acc_ref, tot_ref, wrap_ref, carry_ref, *, step, blocks, ups,
 ):
     here = place_ref[0]
     acc_ref[...] = acc_in[...]
     tot_ref[...] = tot_in[...]
     wrap_ref[...] = wrap_in[...]
     carry_ref[...] = carry_in[...]
-    if step < blocks // 2:
+    if step <= ups:
 
         @pl.when(here >= step)
         def _():
@@ -316,11 +321,22 @@
             tot_ref[...] += total
             entering_state(up_ref, tab_ref, carry_ref, step - 1)
 
-    @pl.when(here >= blocks - step)
-    def _():
-        out, total = score_block(q_ref, down_ref, later_ref, False)
-        wrap_ref[...] = wrap_ref[...] * jnp.exp(-total) + out
-        entering_state(down_ref, tab_ref, carry_ref, blocks - 1 - step)
+    if step < blocks - ups:
+
+        @pl.when(here >= blocks - step)
+        def _():
+            out, total = score_block(q_ref, down_ref, later_ref, False)
+            wrap_ref[...] = wrap_ref[...] * jnp.exp(-total) + out
+            entering_state(down_ref, tab_ref, carry_ref, blocks - 1 - step)
+
+
+def last_kernel(*refs, **sizes):
+    ins, (rest, out_ref, acc_ref, tot_ref, wrap_ref, carry_ref, states_ref) = (
+        refs[:10],
+        (refs[10:14], *refs[14:]),
+    )
+    step_kernel(*ins, acc_ref, tot_ref, wrap_ref, carry_ref, **sizes)
+    finish_kernel(acc_ref, tot_ref, wrap_ref, carry_ref, *rest, out_ref, states_ref)
 
 
 def finish_kernel(
@@ -411,6 +427,7 @@
         norm_kernel,
         shape((4, *tokens.shape), BF16),
         (tokens, norm_gain.reshape(1, -1)),
+        limit=60,
     )
     mine = lax.all_to_all(copies, "tp_0", 0, 0, tiled=True).reshape(4 * piece, -1)
 
@@ -477,13 +494,14 @@
     up = down = payload
     half = blocks // 2
     for step in range(1, half + 1):
+        up = lax.ppermute(up, "sp", [(i - 1, i) for i in range(step, blocks)])
         if step < half:
-            up = lax.ppermute(up, "sp", [(i - 1, i) for i in range(step, blocks)])
-        down = lax.ppermute(
-            down, "sp", [((j - step + 1) % blocks, (j - step) % blocks) for j in range(half)]
-        )
+            hops = [((j - step + 1) % blocks, (j - step) % blocks) for j in range(half - 1)]
+            down = lax.ppermute(down, "sp", hops)
+        if step == half:
+            break
         acc, tot, wrap, carry = call(
-            lambda *refs, step=step: step_kernel(*refs, step=step, blocks=blocks),
+            lambda *refs, step=step: step_kernel(*refs, step=step, blocks=blocks, ups=half),
             (shape((rows, 128)), shape((rows, 128)), shape((rows, 128)), shape(carry.shape)),
             (place, q, later, tab, up, down, acc, tot, wrap, carry),
             smem=1,
@@ -496,22 +514,33 @@
         if step == half - 1:
             acc, w_out_mine = lax.optimization_barrier((acc, w_out_mine))
             w_out_other = lax.ppermute(w_out_mine, "tp_1", [(0, 1), (1, 0)])
+    state = [shape((rows, 128)), shape((rows, 128)), shape((rows, 128)), shape(carry.shape)]
     both = call(
-        finish_kernel,
+        lambda *refs: last_kernel(*refs, step=half, blocks=blocks, ups=half),
         shape((rows, 2 * channels), BF16),
-        (acc, tot, wrap, carry, y_local, chunk, wide, reads),
-        scratch=(pltpu.VMEM((rows, 2 * width), F32),),
+        (place, q, later, tab, up, down, acc, tot, wrap, carry, y_local, chunk, wide, reads),
+        scratch=[pltpu.VMEM(s.shape, F32) for s in state]
+        + [pltpu.VMEM((rows, 2 * width), F32)],
+        smem=1,
         flops=3 * 10**9,
     )
     parts = lax.all_to_all(both.reshape(8, piece, -1), TP, 0, 0, tiled=True)
-    return call(
+    columns = w_out.shape[1]
+    return pl.pallas_call(
         merge_kernel,
-        shape((piece, w_out.shape[1]), BF16),
-        (place, parts, w_out_mine, w_out_other),
-        smem=1,
-        flops=10**9,
-        limit=MERGE_LIMIT,
-    )
+        out_shape=shape((piece, columns), BF16),
+        grid=(4,),
+        in_specs=[
+            SMEM,
+            VMEM,
+            pl.BlockSpec((1, w_out.shape[0], columns), lambda a: (a, 0, 0)),
+            VMEM,
+        ],
+        out_specs=pl.BlockSpec((piece, columns), lambda a: (0, 0)),
+        scratch_shapes=[pltpu.VMEM((piece, columns), F32)],
+        compiler_params=pltpu.CompilerParams(vmem_limit_bytes=16 * 2**20),
+        cost_estimate=pl.CostEstimate(flops=10**9, bytes_accessed=10**7, transcendentals=0),
+    )(place, parts, w_out_mine, w_out_other)
 
 
 def solution(mesh):

time: 140 us -> 135 us (0.964)
  the two profiles are of different devices: /device:TPU:1 before, /device:TPU:408 now
where the time goes in v1:
time: 135 us; the launch traced here: 134 us
  starting transfers between devices  47 us (35%)
  Pallas kernels  34.3 us (25%)
  waiting for transfers between devices  29.4 us (22%)
  blocking collectives  11 us (8%)
  other arithmetic  5.89 us (4%)
  local copies, waits for them, and re-layouts  5.71 us (4%)
    pallas_call x13, Pallas kernels, call(): pl.pallas_call(kernel, out_shape=outs, in_specs=[SMEM] * smem + [VMEM] *...  29.5 us
    ppermute x8, waiting for transfers between devices, on_device(): up = lax.ppermute(up, 'sp', [(i - 1, i) for i in range(step, blocks)])  27.1 us
    ppermute x8, starting transfers between devices, on_device(): up = lax.ppermute(up, 'sp', [(i - 1, i) for i in range(step, blocks)])  19.3 us
    ppermute x7, starting transfers between devices, on_device(): down = lax.ppermute(down, 'sp', hops)  14.7 us
    all_to_all x1, blocking collectives, on_device(): parts = lax.all_to_all(both.reshape(8, piece, -1), TP, 0, 0, tiled=True)  11 us
    all_to_all x1, starting transfers between devices, on_device(): w_out_mine = lax.all_to_all(w_out_copies, 'tp_0', 0, 0, tiled=True)  4.91 us
    pallas_call x1, Pallas kernels, on_device(): pl.pallas_call(merge_kernel, out_shape=shape((piece, columns), BF16), gri...  4.74 us
    all_to_all x1, starting transfers between devices, on_device(): lax.all_to_all(copies, 'tp_0', 0, 0, tiled=True).reshape(4 * piece, -1)  4.29 us
  transfers between devices with their start and end apart: 19, of which 7 were waited for; matrix products, arithmetic and copies ran while one was open for 9% of the time, Pallas kernels for 18%

profile of v1, /device:TPU:408, one launch (start us, length us, event | category | flops | bytes accessed | tf_op | source)
XLA Modules:
  0.0 133.7 jit_solution(169115919658702387)
XLA Ops:
  0.0 2.0 %shard_map.181 = bf16[4,48,2048]{2,1,0:T(8,128)(2,1)} custom-call(bf16[48,2048]{1,0:T(8,128)(2,1)} %tokens_ref.1, f32[1,2048]{1,0:T(1,128)} %bitcast.19), custom_call_target="tpu_custom_call" | custom-call | flops 1 | bytes 1000000 | tf_op jit(solution)/shard_map/pallas_call | solution.py:381
  2.0 4.3 %all-to-all-start = ((bf16[4,48,2048]{2,1,0:T(8,128)(2,1)}), bf16[4,48,2048]{2,1,0:T(8,128)(2,1)S(1)}, u32[]{:S(2)}, u32[]{:S(2)}) async-start(bf16[4,48,2048]{2,1,0:T(8,128)(2,1)} %shard_map.181), calls=%async_computation | async-start | bytes 1572864 | tf_op jit(solution)/shard_map/all_to_all | solution.py:432
  6.3 0.7 exp.3
  6.9 0.7 tile.4
  7.6 0.1 reshape_tile.6.qg_ref
  7.7 0.7 tile.5
  8.3 0.1 reshape_tile.7.kg_ref
  8.4 0.7 reshape.37
  9.1 0.8 fusion
  9.9 0.1 stack_reshape.7
  10.0 0.1 stack_reshape.6
  10.1 0.9 subtract_bitcast_fusion
  11.0 0.1 reshape.33
  11.1 0.1 reshape.34
  11.2 1.0 maximum_maximum_fusion.refs_4_.refs_13_
  12.3 0.1 pad_add_fusion.place_ref.refs_0_
  12.4 1.3 pad_maximum_fusion.1
  13.7 1.7 %pad_maximum_fusion.w_ref = bf16[2048,512]{1,0:T(8,128)(2,1)S(1)} fusion(bf16[2048,128]{1,0:T(8,128)(2,1)} %param.24, bf16[2048,128]{1,0:T(8,128)(2,1)} %param.23, bf16[2048,128]{1,0:T(8,128)(2,1)} %param.22, bf16[2048,128]{1,0:T(8,128)(2,1)} %param.21), kind=kLoop, calls=%fused_computation | loop fusion | flops 8388608 | bytes 4194304 | tf_op jit(solution)/shard_map/concatenate | solution.py:434
  15.4 2.5 %broadcast_in_dim.6 = bf16[4,256,2048]{2,1,0:T(8,128)(2,1)} broadcast(bf16[256,2048]{1,0:T(8,128)(2,1)S(1)} %pad_maximum_fusion.1), dimensions={1,2} | broadcast | bytes 5242880 | tf_op jit(solution)/shard_map/broadcast_in_dim | solution.py:436
  17.9 0.1 shard_map.182
  18.0 0.6 all-to-all-done
  18.6 1.9 %collective-permute-start = (bf16[192,2048]{1,0:T(8,128)(2,1)S(1)}, bf16[192,2048]{1,0:T(8,128)(2,1)S(1)}, u32[]{:S(2)}, u32[]{:S(2)}) collective-permute-start(bf16[192,2048]{1,0:T(8,128)(2,1)S(1)} %bitcast.13), channel_id=1, source_target_pairs={{0,1},{1,0},{2,3},{3,2},{4,5},{5,4},{6,7},{7,6},{8,9},{9,8},{10,11... | collective-permute-start | bytes 2359304 | tf_op jit(solution)/shard_map/ppermute | solution.py:466
  20.5 0.6 shard_map.183.found_ref
  21.1 0.0 copy-start
  21.1 1.6 %collective-permute-done.other_ref = bf16[192,2048]{1,0:T(8,128)(2,1)S(1)} collective-permute-done((bf16[192,2048]{1,0:T(8,128)(2,1)S(1)}, bf16[192,2048]{1,0:T(8,128)(2,1)S(1)}, u32[]{:S(2)}, u32[]{:S(2)}) %collective-permute-start) | collective-permute-done | bytes 786464 | tf_op jit(solution)/shard_map/ppermute | solution.py:466
  22.7 2.2 %shard_map.184 = (bf16[2,384,128]{2,1,0:T(8,128)(2,1)S(1)}, bf16[400,256]{1,0:T(8,128)(2,1)S(1)}, bf16[384,128]{1,0:T(8,128)(2,1)S(1)}, f32[8,1024]{1,0:T(8,128)S(1)}) custom-call(s32[2]{0:T(128)S(1)} %pad_add_fusion.place_ref.refs_0_, bf16[192,512]{1,0:T(8,128)(2,1)S(1)} %shard_map.183.found_ref, bf16[192,2048]{1,0:T(8,128)(2,1)S(1)} %collective-permute-done.other_ref, ...), custom_call_target="tpu_custom_call" | custom-call | flops 4000000000 | bytes 1000000 | tf_op jit(solution)/shard_map/pallas_call | solution.py:381
  25.0 0.7 collective-permute-start.9
  25.7 2.9 %collective-permute-start.1 = (bf16[400,256]{1,0:T(8,128)(2,1)S(1)}, bf16[400,256]{1,0:T(8,128)(2,1)S(1)}, u32[]{:S(2)}, u32[]{:S(2)}) collective-permute-start(bf16[400,256]{1,0:T(8,128)(2,1)S(1)} %get-tuple-element.79.payload_ref), channel_id=1, source_target_pairs={{0,32},{32,64},{64,96},{96,128},{128,160},{160,192},{192,224},{224... | collective-permute-start | bytes 614408 | tf_op jit(solution)/shard_map/ppermute | solution.py:497
  28.6 2.7 %shard_map.185 = (f32[384,128]{1,0:T(8,128)S(1)}, f32[384,128]{1,0:T(8,128)S(1)}, f32[384,128]{1,0:T(8,128)S(1)}) custom-call(bf16[2,384,128]{2,1,0:T(8,128)(2,1)S(1)} %get-tuple-element.76.q_ref.refs_1_, bf16[400,256]{1,0:T(8,128)(2,1)S(1)} %get-tuple-element.79.payload_ref, bf16[384,384]{1,0:T(8,128)(2,1)S(1)} %get-tuple-element.77.later_ref.refs_2_, ...), custom_call_target="tpu_custom_call" | custom-call | flops 4000000000 | bytes 1000000 | tf_op jit(solution)/shard_map/pallas_call | solution.py:381
  31.3 4.6 %collective-permute-done.1.refs_4_ = bf16[400,256]{1,0:T(8,128)(2,1)S(1)} collective-permute-done((bf16[400,256]{1,0:T(8,128)(2,1)S(1)}, bf16[400,256]{1,0:T(8,128)(2,1)S(1)}, u32[]{:S(2)}, u32[]{:S(2)}) %collective-permute-start.1) | collective-permute-done | bytes 204832 | tf_op jit(solution)/shard_map/ppermute | solution.py:497
  35.9 1.9 %shard_map.186 = (f32[384,128]{1,0:T(8,128)S(1)}, f32[384,128]{1,0:T(8,128)S(1)}, f32[384,128]{1,0:T(8,128)S(1)}, f32[8,256]{1,0:T(8,128)S(1)}) custom-call(s32[2]{0:T(128)S(1)} %pad_add_fusion.place_ref.refs_0_, bf16[2,384,128]{2,1,0:T(8,128)(2,1)S(1)} %get-tuple-element.76.q_ref.refs_1_, ...), custom_call_target="tpu_custom_call", output_to_operand_aliasing={{0}: (6, {}), {1}: (7, {}), {2}: (8, {}), {3}: (9, {})} | custom-call | flops 3000000000 | bytes 1000000 | tf_op jit(solution)/shard_map/pallas_call | solution.py:381
  37.8 4.9 %all-to-all-start.1 = ((bf16[4,256,2048]{2,1,0:T(8,128)(2,1)}), bf16[4,256,2048]{2,1,0:T(8,128)(2,1)}, u32[]{:S(2)}, u32[]{:S(2)}) async-start(bf16[4,256,2048]{2,1,0:T(8,128)(2,1)} %broadcast_in_dim.6), calls=%async_computation.1 | async-start | bytes 8388608 | tf_op jit(solution)/shard_map/all_to_all | solution.py:513
  42.7 0.7 collective-permute-start.10
  43.4 1.9 %collective-permute-start.2 = (bf16[400,256]{1,0:T(8,128)(2,1)S(1)}, bf16[400,256]{1,0:T(8,128)(2,1)S(1)}, u32[]{:S(2)}, u32[]{:S(2)}) collective-permute-start(bf16[400,256]{1,0:T(8,128)(2,1)S(1)} %collective-permute-done.1.refs_4_), channel_id=1, source_target_pairs={{32,64},{64,96},{96,128},{128,160},{160,192},{192,224},{224,256},{... | collective-permute-start | bytes 614408 | tf_op jit(solution)/shard_map/ppermute | solution.py:497
  45.4 0.7 collective-permute-start.11
  46.0 6.7 %collective-permute-done.2.refs_4_ = bf16[400,256]{1,0:T(8,128)(2,1)S(1)} collective-permute-done((bf16[400,256]{1,0:T(8,128)(2,1)S(1)}, bf16[400,256]{1,0:T(8,128)(2,1)S(1)}, u32[]{:S(2)}, u32[]{:S(2)}) %collective-permute-start.2) | collective-permute-done | bytes 204832 | tf_op jit(solution)/shard_map/ppermute | solution.py:497
  52.8 1.9 %collective-permute-start.3 = (bf16[400,256]{1,0:T(8,128)(2,1)S(1)}, bf16[400,256]{1,0:T(8,128)(2,1)S(1)}, u32[]{:S(2)}, u32[]{:S(2)}) collective-permute-start(bf16[400,256]{1,0:T(8,128)(2,1)S(1)} %collective-permute-done.2.refs_4_), channel_id=1, source_target_pairs={{64,96},{96,128},{128,160},{160,192},{192,224},{224,256},{256,288}... | collective-permute-start | bytes 614408 | tf_op jit(solution)/shard_map/ppermute | solution.py:497
  54.7 1.9 %shard_map.187 = (f32[384,128]{1,0:T(8,128)S(1)}, f32[384,128]{1,0:T(8,128)S(1)}, f32[384,128]{1,0:T(8,128)S(1)}, f32[8,256]{1,0:T(8,128)S(1)}) custom-call(s32[2]{0:T(128)S(1)} %pad_add_fusion.place_ref.refs_0_, bf16[2,384,128]{2,1,0:T(8,128)(2,1)S(1)} %get-tuple-element.76.q_ref.refs_1_, ...), custom_call_target="tpu_custom_call", output_to_operand_aliasing={{0}: (6, {}), {1}: (7, {}), {2}: (8, {}), {3}: (9, {})} | custom-call | flops 3000000000 | bytes 1000000 | tf_op jit(solution)/shard_map/pallas_call | solution.py:381
  56.6 0.0 collective-permute-done.11.refs_5_
  56.6 1.3 collective-permute-start.12
  57.9 3.7 %collective-permute-done.3.refs_4_ = bf16[400,256]{1,0:T(8,128)(2,1)S(1)} collective-permute-done((bf16[400,256]{1,0:T(8,128)(2,1)S(1)}, bf16[400,256]{1,0:T(8,128)(2,1)S(1)}, u32[]{:S(2)}, u32[]{:S(2)}) %collective-permute-start.3) | collective-permute-done | bytes 204832 | tf_op jit(solution)/shard_map/ppermute | solution.py:497
  61.6 1.9 %collective-permute-start.4 = (bf16[400,256]{1,0:T(8,128)(2,1)S(1)}, bf16[400,256]{1,0:T(8,128)(2,1)S(1)}, u32[]{:S(2)}, u32[]{:S(2)}) collective-permute-start(bf16[400,256]{1,0:T(8,128)(2,1)S(1)} %collective-permute-done.3.refs_4_), channel_id=1, source_target_pairs={{96,128},{128,160},{160,192},{192,224},{224,256},{256,288},{288,32... | collective-permute-start | bytes 614408 | tf_op jit(solution)/shard_map/ppermute | solution.py:497
  63.5 2.1 %shard_map.188 = (f32[384,128]{1,0:T(8,128)S(1)}, f32[384,128]{1,0:T(8,128)S(1)}, f32[384,128]{1,0:T(8,128)S(1)}, f32[8,256]{1,0:T(8,128)S(1)}) custom-call(s32[2]{0:T(128)S(1)} %pad_add_fusion.place_ref.refs_0_, bf16[2,384,128]{2,1,0:T(8,128)(2,1)S(1)} %get-tuple-element.76.q_ref.refs_1_, ...), custom_call_target="tpu_custom_call", output_to_operand_aliasing={{0}: (6, {}), {1}: (7, {}), {2}: (8, {}), {3}: (9, {})} | custom-call | flops 3000000000 | bytes 1000000 | tf_op jit(solution)/shard_map/pallas_call | solution.py:381
  65.6 0.0 collective-permute-done.12.refs_5_
  65.7 5.2 %collective-permute-start.13 = (bf16[400,256]{1,0:T(8,128)(2,1)S(1)}, bf16[400,256]{1,0:T(8,128)(2,1)S(1)}, u32[]{:S(2)}, u32[]{:S(2)}) collective-permute-start(bf16[400,256]{1,0:T(8,128)(2,1)S(1)} %collective-permute-done.12.refs_5_), channel_id=1, source_target_pairs={{384,352},{416,384},{448,416},{480,448},{0,480},{32,0},{64,32},{38... | collective-permute-start | bytes 614408 | tf_op jit(solution)/shard_map/ppermute | solution.py:500
  70.8 0.0 collective-permute-done.4.refs_4_
  70.8 3.2 %collective-permute-start.5 = (bf16[400,256]{1,0:T(8,128)(2,1)S(1)}, bf16[400,256]{1,0:T(8,128)(2,1)S(1)}, u32[]{:S(2)}, u32[]{:S(2)}) collective-permute-start(bf16[400,256]{1,0:T(8,128)(2,1)S(1)} %collective-permute-done.4.refs_4_), channel_id=1, source_target_pairs={{128,160},{160,192},{192,224},{224,256},{256,288},{288,320},{320,3... | collective-permute-start | bytes 614408 | tf_op jit(solution)/shard_map/ppermute | solution.py:497
  74.1 3.2 %shard_map.189 = (f32[384,128]{1,0:T(8,128)S(1)}, f32[384,128]{1,0:T(8,128)S(1)}, f32[384,128]{1,0:T(8,128)S(1)}, f32[8,256]{1,0:T(8,128)S(1)}) custom-call(s32[2]{0:T(128)S(1)} %pad_add_fusion.place_ref.refs_0_, bf16[2,384,128]{2,1,0:T(8,128)(2,1)S(1)} %get-tuple-element.76.q_ref.refs_1_, ...), custom_call_target="tpu_custom_call", output_to_operand_aliasing={{0}: (6, {}), {1}: (7, {}), {2}: (8, {}), {3}: (9, {})} | custom-call | flops 3000000000 | bytes 1000000 | tf_op jit(solution)/shard_map/pallas_call | solution.py:381
  77.3 0.0 collective-permute-done.13.refs_5_
  77.3 2.5 %collective-permute-start.14 = (bf16[400,256]{1,0:T(8,128)(2,1)S(1)}, bf16[400,256]{1,0:T(8,128)(2,1)S(1)}, u32[]{:S(2)}, u32[]{:S(2)}) collective-permute-start(bf16[400,256]{1,0:T(8,128)(2,1)S(1)} %collective-permute-done.13.refs_5_), channel_id=1, source_target_pairs={{352,320},{384,352},{416,384},{448,416},{480,448},{0,480},{32,0},{... | collective-permute-start | bytes 614408 | tf_op jit(solution)/shard_map/ppermute | solution.py:500
  79.8 0.0 collective-permute-done.5.refs_4_
  79.8 3.3 %collective-permute-start.6 = (bf16[400,256]{1,0:T(8,128)(2,1)S(1)}, bf16[400,256]{1,0:T(8,128)(2,1)S(1)}, u32[]{:S(2)}, u32[]{:S(2)}) collective-permute-start(bf16[400,256]{1,0:T(8,128)(2,1)S(1)} %collective-permute-done.5.refs_4_), channel_id=1, source_target_pairs={{160,192},{192,224},{224,256},{256,288},{288,320},{320,352},{352,3... | collective-permute-start | bytes 614408 | tf_op jit(solution)/shard_map/ppermute | solution.py:497
  83.2 3.2 %shard_map.190 = (f32[384,128]{1,0:T(8,128)S(1)}, f32[384,128]{1,0:T(8,128)S(1)}, f32[384,128]{1,0:T(8,128)S(1)}, f32[8,256]{1,0:T(8,128)S(1)}) custom-call(s32[2]{0:T(128)S(1)} %pad_add_fusion.place_ref.refs_0_, bf16[2,384,128]{2,1,0:T(8,128)(2,1)S(1)} %get-tuple-element.76.q_ref.refs_1_, ...), custom_call_target="tpu_custom_call", output_to_operand_aliasing={{0}: (6, {}), {1}: (7, {}), {2}: (8, {}), {3}: (9, {})} | custom-call | flops 3000000000 | bytes 1000000 | tf_op jit(solution)/shard_map/pallas_call | solution.py:381
  86.4 3.7 %collective-permute-start.15 = (bf16[400,256]{1,0:T(8,128)(2,1)S(1)}, bf16[400,256]{1,0:T(8,128)(2,1)S(1)}, u32[]{:S(2)}, u32[]{:S(2)}) collective-permute-start(bf16[400,256]{1,0:T(8,128)(2,1)S(1)} %collective-permute-done.14.refs_5_), channel_id=1, source_target_pairs={{320,288},{352,320},{384,352},{416,384},{448,416},{480,448},{0,480... | collective-permute-start | bytes 614408 | tf_op jit(solution)/shard_map/ppermute | solution.py:500
  90.2 2.1 %collective-permute-start.7 = (bf16[400,256]{1,0:T(8,128)(2,1)S(1)}, bf16[400,256]{1,0:T(8,128)(2,1)S(1)}, u32[]{:S(2)}, u32[]{:S(2)}) collective-permute-start(bf16[400,256]{1,0:T(8,128)(2,1)S(1)} %collective-permute-done.6.refs_4_), channel_id=1, source_target_pairs={{192,224},{224,256},{256,288},{288,320},{320,352},{352,384},{384,4... | collective-permute-start | bytes 614408 | tf_op jit(solution)/shard_map/ppermute | solution.py:497
  92.3 3.2 %shard_map.191 = (f32[384,128]{1,0:T(8,128)S(1)}, f32[384,128]{1,0:T(8,128)S(1)}, f32[384,128]{1,0:T(8,128)S(1)}, f32[8,256]{1,0:T(8,128)S(1)}) custom-call(s32[2]{0:T(128)S(1)} %pad_add_fusion.place_ref.refs_0_, bf16[2,384,128]{2,1,0:T(8,128)(2,1)S(1)} %get-tuple-element.76.q_ref.refs_1_, ...), custom_call_target="tpu_custom_call", output_to_operand_aliasing={{0}: (6, {}), {1}: (7, {}), {2}: (8, {}), {3}: (9, {})} | custom-call | flops 3000000000 | bytes 1000000 | tf_op jit(solution)/shard_map/pallas_call | solution.py:381
  95.6 3.5 %collective-permute-done.7.refs_4_ = bf16[400,256]{1,0:T(8,128)(2,1)S(1)} collective-permute-done((bf16[400,256]{1,0:T(8,128)(2,1)S(1)}, bf16[400,256]{1,0:T(8,128)(2,1)S(1)}, u32[]{:S(2)}, u32[]{:S(2)}) %collective-permute-start.7) | collective-permute-done | bytes 204832 | tf_op jit(solution)/shard_map/ppermute | solution.py:497
  99.0 3.2 %shard_map.192 = (f32[384,128]{1,0:T(8,128)S(1)}, f32[384,128]{1,0:T(8,128)S(1)}, f32[384,128]{1,0:T(8,128)S(1)}, f32[8,256]{1,0:T(8,128)S(1)}) custom-call(s32[2]{0:T(128)S(1)} %pad_add_fusion.place_ref.refs_0_, bf16[2,384,128]{2,1,0:T(8,128)(2,1)S(1)} %get-tuple-element.76.q_ref.refs_1_, ...), custom_call_target="tpu_custom_call", output_to_operand_aliasing={{0}: (6, {}), {1}: (7, {}), {2}: (8, {}), {3}: (9, {})} | custom-call | flops 3000000000 | bytes 1000000 | tf_op jit(solution)/shard_map/pallas_call | solution.py:381
  102.3 1.9 %collective-permute-start.16 = (bf16[4,256,2048]{2,1,0:T(8,128)(2,1)}, bf16[4,256,2048]{2,1,0:T(8,128)(2,1)S(1)}, u32[]{:S(2)}, u32[]{:S(2)}) collective-permute-start(bf16[4,256,2048]{2,1,0:T(8,128)(2,1)} %all-to-all-done.1.mine_ref), channel_id=1, source_target_pairs={{0,1},{1,0},{2,3},{3,2},{4,5},{5,4},{6,7},{7,6},{8,9},{9,8},{10,11... | collective-permute-start | bytes 12582920 | tf_op jit(solution)/shard_map/ppermute | solution.py:516
  104.2 1.9 %collective-permute-start.8 = (bf16[400,256]{1,0:T(8,128)(2,1)S(1)}, bf16[400,256]{1,0:T(8,128)(2,1)S(1)}, u32[]{:S(2)}, u32[]{:S(2)}) collective-permute-start(bf16[400,256]{1,0:T(8,128)(2,1)S(1)} %collective-permute-done.7.refs_4_), channel_id=1, source_target_pairs={{224,256},{256,288},{288,320},{320,352},{352,384},{384,416},{416,4... | collective-permute-start | bytes 614408 | tf_op jit(solution)/shard_map/ppermute | solution.py:497
  106.1 8.7 %collective-permute-done.8.refs_4_ = bf16[400,256]{1,0:T(8,128)(2,1)S(1)} collective-permute-done((bf16[400,256]{1,0:T(8,128)(2,1)S(1)}, bf16[400,256]{1,0:T(8,128)(2,1)S(1)}, u32[]{:S(2)}, u32[]{:S(2)}) %collective-permute-start.8) | collective-permute-done | bytes 204832 | tf_op jit(solution)/shard_map/ppermute | solution.py:497
  114.8 3.1 %shard_map.193 = bf16[384,256]{1,0:T(8,128)(2,1)S(1)} custom-call(s32[2]{0:T(128)S(1)} %pad_add_fusion.place_ref.refs_0_, bf16[2,384,128]{2,1,0:T(8,128)(2,1)S(1)} %get-tuple-element.76.q_ref.refs_1_, bf16[384,384]{1,0:T(8,128)(2,1)S(1)} %get-tuple-element.77.later_ref.refs_2_, f32[64,256]{1,0:T(8,128)S(1)} %get-tuple-element.78.refs_3_, ...), custom_call_target="tpu_custom_call" | custom-call | flops 3000000000 | bytes 1000000 | tf_op jit(solution)/shard_map/pallas_call | solution.py:381
  117.9 11.0 %all_to_all.15.parts_ref = bf16[8,48,256]{2,1,0:T(8,128)(2,1)S(1)} all-to-all(bf16[8,48,256]{2,1,0:T(8,128)(2,1)S(1)} %bitcast.15), channel_id=1, replica_groups=mesh['sp'=16,'fs'=4,'tp_0'=4,'tp_1'=2] {'tp_0','tp_1'}, dimensions={0} | all-to-all | bytes 393216 | tf_op jit(solution)/shard_map/all_to_all | solution.py:527
  128.9 4.7 %shard_map.194 = bf16[48,2048]{1,0:T(8,128)(2,1)} custom-call(s32[2]{0:T(128)S(1)} %pad_add_fusion.place_ref.refs_0_, bf16[8,48,256]{2,1,0:T(8,128)(2,1)S(1)} %all_to_all.15.parts_ref, bf16[4,256,2048]{2,1,0:T(8,128)(2,1)} %all-to-all-done.1.mine_ref, bf16[4,256,2048]{2,1,0:T(8,128)(2,1)S(1)} %collective-permute-done.16.other_ref), custom_call_target="tpu_custom_call" | custom-call | flops 1000000000 | bytes 10000000 | tf_op jit(solution)/shard_map/pallas_call | solution.py:529
  (15 shorter events, 0.1 us)
Async XLA Ops:
  2.0 16.6 %all-to-all-start = ((bf16[4,48,2048]{2,1,0:T(8,128)(2,1)}), bf16[4,48,2048]{2,1,0:T(8,128)(2,1)S(1)}, u32[]{:S(2)}, u32[]{:S(2)}) async-start(bf16[4,48,2048]{2,1,0:T(8,128)(2,1)} %shard_map.181), calls=%async_computation | async-start | bytes 1572864 | tf_op jit(solution)/shard_map/all_to_all | solution.py:432
  18.6 4.2 %collective-permute-start = (bf16[192,2048]{1,0:T(8,128)(2,1)S(1)}, bf16[192,2048]{1,0:T(8,128)(2,1)S(1)}, u32[]{:S(2)}, u32[]{:S(2)}) collective-permute-start(bf16[192,2048]{1,0:T(8,128)(2,1)S(1)} %bitcast.13), channel_id=1, source_target_pairs={{0,1},{1,0},{2,3},{3,2},{4,5},{5,4},{6,7},{7,6},{8,9},{9,8},{10,11... | collective-permute-start | bytes 2359304 | tf_op jit(solution)/shard_map/ppermute | solution.py:466
  21.1 7.5 %copy-start = (f32[128]{0:T(128)S(1)}, f32[128]{0:T(128)}, u32[]{:S(2)}) copy-start(f32[128]{0:T(128)} %param.35) | copy-start | bytes 1540
  25.0 6.3 %collective-permute-start.9 = (bf16[400,256]{1,0:T(8,128)(2,1)S(1)}, bf16[400,256]{1,0:T(8,128)(2,1)S(1)}, u32[]{:S(2)}, u32[]{:S(2)}) collective-permute-start(bf16[400,256]{1,0:T(8,128)(2,1)S(1)} %get-tuple-element.79.payload_ref), channel_id=1, source_target_pairs={{0,480},{32,0},{64,32},{96,64},{128,96},{160,128},{192,160},{1,481... | collective-permute-start | bytes 614408 | tf_op jit(solution)/shard_map/ppermute | solution.py:500
  25.7 10.2 %collective-permute-start.1 = (bf16[400,256]{1,0:T(8,128)(2,1)S(1)}, bf16[400,256]{1,0:T(8,128)(2,1)S(1)}, u32[]{:S(2)}, u32[]{:S(2)}) collective-permute-start(bf16[400,256]{1,0:T(8,128)(2,1)S(1)} %get-tuple-element.79.payload_ref), channel_id=1, source_target_pairs={{0,32},{32,64},{64,96},{96,128},{128,160},{160,192},{192,224},{224... | collective-permute-start | bytes 614408 | tf_op jit(solution)/shard_map/ppermute | solution.py:497
  37.8 64.4 %all-to-all-start.1 = ((bf16[4,256,2048]{2,1,0:T(8,128)(2,1)}), bf16[4,256,2048]{2,1,0:T(8,128)(2,1)}, u32[]{:S(2)}, u32[]{:S(2)}) async-start(bf16[4,256,2048]{2,1,0:T(8,128)(2,1)} %broadcast_in_dim.6), calls=%async_computation.1 | async-start | bytes 8388608 | tf_op jit(solution)/shard_map/all_to_all | solution.py:513
  42.7 2.6 %collective-permute-start.10 = (bf16[400,256]{1,0:T(8,128)(2,1)S(1)}, bf16[400,256]{1,0:T(8,128)(2,1)S(1)}, u32[]{:S(2)}, u32[]{:S(2)}) collective-permute-start(bf16[400,256]{1,0:T(8,128)(2,1)S(1)} %collective-permute-done.9.refs_5_), channel_id=1, source_target_pairs={{480,448},{0,480},{32,0},{64,32},{96,64},{128,96},{160,128},{481,4... | collective-permute-start | bytes 614408 | tf_op jit(solution)/shard_map/ppermute | solution.py:500
  43.4 9.4 %collective-permute-start.2 = (bf16[400,256]{1,0:T(8,128)(2,1)S(1)}, bf16[400,256]{1,0:T(8,128)(2,1)S(1)}, u32[]{:S(2)}, u32[]{:S(2)}) collective-permute-start(bf16[400,256]{1,0:T(8,128)(2,1)S(1)} %collective-permute-done.1.refs_4_), channel_id=1, source_target_pairs={{32,64},{64,96},{96,128},{128,160},{160,192},{192,224},{224,256},{... | collective-permute-start | bytes 614408 | tf_op jit(solution)/shard_map/ppermute | solution.py:497
  45.4 11.3 %collective-permute-start.11 = (bf16[400,256]{1,0:T(8,128)(2,1)S(1)}, bf16[400,256]{1,0:T(8,128)(2,1)S(1)}, u32[]{:S(2)}, u32[]{:S(2)}) collective-permute-start(bf16[400,256]{1,0:T(8,128)(2,1)S(1)} %collective-permute-done.10.refs_5_), channel_id=1, source_target_pairs={{448,416},{480,448},{0,480},{32,0},{64,32},{96,64},{128,96},{449,4... | collective-permute-start | bytes 614408 | tf_op jit(solution)/shard_map/ppermute | solution.py:500
  52.8 8.9 %collective-permute-start.3 = (bf16[400,256]{1,0:T(8,128)(2,1)S(1)}, bf16[400,256]{1,0:T(8,128)(2,1)S(1)}, u32[]{:S(2)}, u32[]{:S(2)}) collective-permute-start(bf16[400,256]{1,0:T(8,128)(2,1)S(1)} %collective-permute-done.2.refs_4_), channel_id=1, source_target_pairs={{64,96},{96,128},{128,160},{160,192},{192,224},{224,256},{256,288}... | collective-permute-start | bytes 614408 | tf_op jit(solution)/shard_map/ppermute | solution.py:497
  56.6 9.0 %collective-permute-start.12 = (bf16[400,256]{1,0:T(8,128)(2,1)S(1)}, bf16[400,256]{1,0:T(8,128)(2,1)S(1)}, u32[]{:S(2)}, u32[]{:S(2)}) collective-permute-start(bf16[400,256]{1,0:T(8,128)(2,1)S(1)} %collective-permute-done.11.refs_5_), channel_id=1, source_target_pairs={{416,384},{448,416},{480,448},{0,480},{32,0},{64,32},{96,64},{417,... | collective-permute-start | bytes 614408 | tf_op jit(solution)/shard_map/ppermute | solution.py:500
  61.6 9.2 %collective-permute-start.4 = (bf16[400,256]{1,0:T(8,128)(2,1)S(1)}, bf16[400,256]{1,0:T(8,128)(2,1)S(1)}, u32[]{:S(2)}, u32[]{:S(2)}) collective-permute-start(bf16[400,256]{1,0:T(8,128)(2,1)S(1)} %collective-permute-done.3.refs_4_), channel_id=1, source_target_pairs={{96,128},{128,160},{160,192},{192,224},{224,256},{256,288},{288,32... | collective-permute-start | bytes 614408 | tf_op jit(solution)/shard_map/ppermute | solution.py:497
  65.7 11.7 %collective-permute-start.13 = (bf16[400,256]{1,0:T(8,128)(2,1)S(1)}, bf16[400,256]{1,0:T(8,128)(2,1)S(1)}, u32[]{:S(2)}, u32[]{:S(2)}) collective-permute-start(bf16[400,256]{1,0:T(8,128)(2,1)S(1)} %collective-permute-done.12.refs_5_), channel_id=1, source_target_pairs={{384,352},{416,384},{448,416},{480,448},{0,480},{32,0},{64,32},{38... | collective-permute-start | bytes 614408 | tf_op jit(solution)/shard_map/ppermute | solution.py:500
  70.8 9.0 %collective-permute-start.5 = (bf16[400,256]{1,0:T(8,128)(2,1)S(1)}, bf16[400,256]{1,0:T(8,128)(2,1)S(1)}, u32[]{:S(2)}, u32[]{:S(2)}) collective-permute-start(bf16[400,256]{1,0:T(8,128)(2,1)S(1)} %collective-permute-done.4.refs_4_), channel_id=1, source_target_pairs={{128,160},{160,192},{192,224},{224,256},{256,288},{288,320},{320,3... | collective-permute-start | bytes 614408 | tf_op jit(solution)/shard_map/ppermute | solution.py:497
  77.3 9.1 %collective-permute-start.14 = (bf16[400,256]{1,0:T(8,128)(2,1)S(1)}, bf16[400,256]{1,0:T(8,128)(2,1)S(1)}, u32[]{:S(2)}, u32[]{:S(2)}) collective-permute-start(bf16[400,256]{1,0:T(8,128)(2,1)S(1)} %collective-permute-done.13.refs_5_), channel_id=1, source_target_pairs={{352,320},{384,352},{416,384},{448,416},{480,448},{0,480},{32,0},{... | collective-permute-start | bytes 614408 | tf_op jit(solution)/shard_map/ppermute | solution.py:500
  79.8 10.3 %collective-permute-start.6 = (bf16[400,256]{1,0:T(8,128)(2,1)S(1)}, bf16[400,256]{1,0:T(8,128)(2,1)S(1)}, u32[]{:S(2)}, u32[]{:S(2)}) collective-permute-start(bf16[400,256]{1,0:T(8,128)(2,1)S(1)} %collective-permute-done.5.refs_4_), channel_id=1, source_target_pairs={{160,192},{192,224},{224,256},{256,288},{288,320},{320,352},{352,3... | collective-permute-start | bytes 614408 | tf_op jit(solution)/shard_map/ppermute | solution.py:497
  86.4 9.1 %collective-permute-start.15 = (bf16[400,256]{1,0:T(8,128)(2,1)S(1)}, bf16[400,256]{1,0:T(8,128)(2,1)S(1)}, u32[]{:S(2)}, u32[]{:S(2)}) collective-permute-start(bf16[400,256]{1,0:T(8,128)(2,1)S(1)} %collective-permute-done.14.refs_5_), channel_id=1, source_target_pairs={{320,288},{352,320},{384,352},{416,384},{448,416},{480,448},{0,480... | collective-permute-start | bytes 614408 | tf_op jit(solution)/shard_map/ppermute | solution.py:500
  90.2 8.9 %collective-permute-start.7 = (bf16[400,256]{1,0:T(8,128)(2,1)S(1)}, bf16[400,256]{1,0:T(8,128)(2,1)S(1)}, u32[]{:S(2)}, u32[]{:S(2)}) collective-permute-start(bf16[400,256]{1,0:T(8,128)(2,1)S(1)} %collective-permute-done.6.refs_4_), channel_id=1, source_target_pairs={{192,224},{224,256},{256,288},{288,320},{320,352},{352,384},{384,4... | collective-permute-start | bytes 614408 | tf_op jit(solution)/shard_map/ppermute | solution.py:497
  102.3 26.7 %collective-permute-start.16 = (bf16[4,256,2048]{2,1,0:T(8,128)(2,1)}, bf16[4,256,2048]{2,1,0:T(8,128)(2,1)S(1)}, u32[]{:S(2)}, u32[]{:S(2)}) collective-permute-start(bf16[4,256,2048]{2,1,0:T(8,128)(2,1)} %all-to-all-done.1.mine_ref), channel_id=1, source_target_pairs={{0,1},{1,0},{2,3},{3,2},{4,5},{5,4},{6,7},{7,6},{8,9},{9,8},{10,11... | collective-permute-start | bytes 12582920 | tf_op jit(solution)/shard_map/ppermute | solution.py:516
  104.2 10.6 %collective-permute-start.8 = (bf16[400,256]{1,0:T(8,128)(2,1)S(1)}, bf16[400,256]{1,0:T(8,128)(2,1)S(1)}, u32[]{:S(2)}, u32[]{:S(2)}) collective-permute-start(bf16[400,256]{1,0:T(8,128)(2,1)S(1)} %collective-permute-done.7.refs_4_), channel_id=1, source_target_pairs={{224,256},{256,288},{288,320},{320,352},{352,384},{384,416},{416,4... | collective-permute-start | bytes 614408 | tf_op jit(solution)/shard_map/ppermute | solution.py:497

commit v2 on v1

--- a/solution.py
+++ b/solution.py
@@ -89,7 +89,7 @@
         total_ref[...] = jnp.zeros_like(total_ref)
 
     total_ref[...] += nn_dot(parts_ref[2 * a + core], mine_ref[0]) + nn_dot(
-        parts_ref[2 * a + 1 - core], other_ref[a]
+        parts_ref[2 * a + 1 - core], other_ref[0]
     )
 
     @pl.when(a == pl.num_programs(0) - 1)
@@ -489,6 +489,8 @@
         scratch=(pltpu.VMEM((rows, 2 * width), F32),),
         flops=4 * 10**9,
     )
+    acc, w_out_copies = lax.optimization_barrier((acc, w_out_copies))
+    w_out_mine = lax.all_to_all(w_out_copies, "tp_0", 0, 0, tiled=True)
     wrap = jnp.zeros((rows, 128), F32)
     carry = jnp.zeros((8, width // 2), F32)
     up = down = payload
@@ -508,10 +510,7 @@
             flops=3 * 10**9,
             aliases={6: 0, 7: 1, 8: 2, 9: 3},
         )
-        if step == 1:
-            acc, w_out_copies = lax.optimization_barrier((acc, w_out_copies))
-            w_out_mine = lax.all_to_all(w_out_copies, "tp_0", 0, 0, tiled=True)
-        if step == half - 1:
+        if step == half - 2:
             acc, w_out_mine = lax.optimization_barrier((acc, w_out_mine))
             w_out_other = lax.ppermute(w_out_mine, "tp_1", [(0, 1), (1, 0)])
     state = [shape((rows, 128)), shape((rows, 128)), shape((rows, 128)), shape(carry.shape)]
@@ -534,7 +533,7 @@
             SMEM,
             VMEM,
             pl.BlockSpec((1, w_out.shape[0], columns), lambda a: (a, 0, 0)),
-            VMEM,
+            pl.BlockSpec((1, w_out.shape[0], columns), lambda a: (a, 0, 0)),
         ],
         out_specs=pl.BlockSpec((piece, columns), lambda a: (0, 0)),
         scratch_shapes=[pltpu.VMEM((piece, columns), F32)],

time: 135 us -> 134 us (level)
    ppermute x7, starting transfers between devices: 14.7 us -> 16.8 us  [on_device(): down = lax.ppermute(down, 'sp', hops)]
    ppermute x8, starting transfers between devices: 19.3 us -> 17.6 us  [on_device(): up = lax.ppermute(up, 'sp', [(i - 1, i) for i in range(step, blocks)])]
  transfers between devices with their start and end apart: 19 -> 19, of which waited for: 7 -> 8; matrix products, arithmetic and copies ran while one was open for 9% -> 9% of each run, Pallas kernels for 18% -> 17%
where the time goes in v2:
time: 134 us; the launch traced here: 133 us
  starting transfers between devices  47.5 us (35%)
  Pallas kernels  34.2 us (26%)
  waiting for transfers between devices  28.5 us (21%)
  blocking collectives  10.7 us (8%)
  other arithmetic  5.89 us (4%)
  local copies, waits for them, and re-layouts  5.71 us (4%)
    pallas_call x13, Pallas kernels, call(): pl.pallas_call(kernel, out_shape=outs, in_specs=[SMEM] * smem + [VMEM] *...  29.5 us
    ppermute x8, waiting for transfers between devices, on_device(): up = lax.ppermute(up, 'sp', [(i - 1, i) for i in range(step, blocks)])  26.3 us
    ppermute x8, starting transfers between devices, on_device(): up = lax.ppermute(up, 'sp', [(i - 1, i) for i in range(step, blocks)])  17.6 us
    ppermute x7, starting transfers between devices, on_device(): down = lax.ppermute(down, 'sp', hops)  16.8 us
    all_to_all x1, blocking collectives, on_device(): parts = lax.all_to_all(both.reshape(8, piece, -1), TP, 0, 0, tiled=True)  10.7 us
    all_to_all x1, starting transfers between devices, on_device(): w_out_mine = lax.all_to_all(w_out_copies, 'tp_0', 0, 0, tiled=True)  4.91 us
    pallas_call x1, Pallas kernels, on_device(): pl.pallas_call(merge_kernel, out_shape=shape((piece, columns), BF16), gri...  4.73 us
    all_to_all x1, starting transfers between devices, on_device(): lax.all_to_all(copies, 'tp_0', 0, 0, tiled=True).reshape(4 * piece, -1)  4.29 us
  transfers between devices with their start and end apart: 19, of which 8 were waited for; matrix products, arithmetic and copies ran while one was open for 9% of the time, Pallas kernels for 17%

profile of v2, /device:TPU:408, one launch (start us, length us, event | category | flops | bytes accessed | tf_op | source)
XLA Modules:
  0.0 133.0 jit_solution(4822007699670098564)
XLA Ops:
  0.0 2.0 %shard_map.181 = bf16[4,48,2048]{2,1,0:T(8,128)(2,1)} custom-call(bf16[48,2048]{1,0:T(8,128)(2,1)} %tokens_ref.1, f32[1,2048]{1,0:T(1,128)} %bitcast.19), custom_call_target="tpu_custom_call" | custom-call | flops 1 | bytes 1000000 | tf_op jit(solution)/shard_map/pallas_call | solution.py:381
  2.0 4.3 %all-to-all-start = ((bf16[4,48,2048]{2,1,0:T(8,128)(2,1)}), bf16[4,48,2048]{2,1,0:T(8,128)(2,1)S(1)}, u32[]{:S(2)}, u32[]{:S(2)}) async-start(bf16[4,48,2048]{2,1,0:T(8,128)(2,1)} %shard_map.181), calls=%async_computation | async-start | bytes 1572864 | tf_op jit(solution)/shard_map/all_to_all | solution.py:432
  6.3 0.7 exp.3
  6.9 0.7 tile.4
  7.6 0.1 reshape_tile.6.qg_ref
  7.7 0.7 tile.5
  8.3 0.1 reshape_tile.7.kg_ref
  8.4 0.7 reshape.37
  9.1 0.8 fusion
  9.9 0.1 stack_reshape.7
  10.0 0.1 stack_reshape.6
  10.1 0.9 subtract_bitcast_fusion
  11.0 0.1 reshape.33
  11.1 0.1 reshape.34
  11.2 1.0 maximum_maximum_fusion.refs_4_.refs_13_
  12.3 0.1 pad_add_fusion.place_ref.refs_0_
  12.4 1.3 pad_maximum_fusion.1
  13.7 1.7 %pad_maximum_fusion.w_ref = bf16[2048,512]{1,0:T(8,128)(2,1)S(1)} fusion(bf16[2048,128]{1,0:T(8,128)(2,1)} %param.24, bf16[2048,128]{1,0:T(8,128)(2,1)} %param.23, bf16[2048,128]{1,0:T(8,128)(2,1)} %param.22, bf16[2048,128]{1,0:T(8,128)(2,1)} %param.21), kind=kLoop, calls=%fused_computation | loop fusion | flops 8388608 | bytes 4194304 | tf_op jit(solution)/shard_map/concatenate | solution.py:434
  15.4 2.5 %broadcast_in_dim.6 = bf16[4,256,2048]{2,1,0:T(8,128)(2,1)} broadcast(bf16[256,2048]{1,0:T(8,128)(2,1)S(1)} %pad_maximum_fusion.1), dimensions={1,2} | broadcast | bytes 5242880 | tf_op jit(solution)/shard_map/broadcast_in_dim | solution.py:436
  17.9 0.1 shard_map.182
  18.0 0.6 all-to-all-done
  18.6 1.9 %collective-permute-start = (bf16[192,2048]{1,0:T(8,128)(2,1)S(1)}, bf16[192,2048]{1,0:T(8,128)(2,1)S(1)}, u32[]{:S(2)}, u32[]{:S(2)}) collective-permute-start(bf16[192,2048]{1,0:T(8,128)(2,1)S(1)} %bitcast.13), channel_id=1, source_target_pairs={{0,1},{1,0},{2,3},{3,2},{4,5},{5,4},{6,7},{7,6},{8,9},{9,8},{10,11... | collective-permute-start | bytes 2359304 | tf_op jit(solution)/shard_map/ppermute | solution.py:466
  20.5 0.6 shard_map.183.found_ref
  21.1 0.0 copy-start
  21.1 1.7 %collective-permute-done.other_ref = bf16[192,2048]{1,0:T(8,128)(2,1)S(1)} collective-permute-done((bf16[192,2048]{1,0:T(8,128)(2,1)S(1)}, bf16[192,2048]{1,0:T(8,128)(2,1)S(1)}, u32[]{:S(2)}, u32[]{:S(2)}) %collective-permute-start) | collective-permute-done | bytes 786464 | tf_op jit(solution)/shard_map/ppermute | solution.py:466
  22.7 2.2 %shard_map.184 = (bf16[2,384,128]{2,1,0:T(8,128)(2,1)S(1)}, bf16[400,256]{1,0:T(8,128)(2,1)S(1)}, bf16[384,128]{1,0:T(8,128)(2,1)S(1)}, f32[8,1024]{1,0:T(8,128)S(1)}) custom-call(s32[2]{0:T(128)S(1)} %pad_add_fusion.place_ref.refs_0_, bf16[192,512]{1,0:T(8,128)(2,1)S(1)} %shard_map.183.found_ref, bf16[192,2048]{1,0:T(8,128)(2,1)S(1)} %collective-permute-done.other_ref, ...), custom_call_target="tpu_custom_call" | custom-call | flops 4000000000 | bytes 1000000 | tf_op jit(solution)/shard_map/pallas_call | solution.py:381
  25.0 2.7 %shard_map.185 = (f32[384,128]{1,0:T(8,128)S(1)}, f32[384,128]{1,0:T(8,128)S(1)}, f32[384,128]{1,0:T(8,128)S(1)}) custom-call(bf16[2,384,128]{2,1,0:T(8,128)(2,1)S(1)} %get-tuple-element.76.q_ref.refs_1_, bf16[400,256]{1,0:T(8,128)(2,1)S(1)} %get-tuple-element.79.payload_ref, bf16[384,384]{1,0:T(8,128)(2,1)S(1)} %get-tuple-element.77.later_ref.refs_2_, ...), custom_call_target="tpu_custom_call" | custom-call | flops 4000000000 | bytes 1000000 | tf_op jit(solution)/shard_map/pallas_call | solution.py:381
  27.7 4.9 %all-to-all-start.1 = ((bf16[4,256,2048]{2,1,0:T(8,128)(2,1)}), bf16[4,256,2048]{2,1,0:T(8,128)(2,1)}, u32[]{:S(2)}, u32[]{:S(2)}) async-start(bf16[4,256,2048]{2,1,0:T(8,128)(2,1)} %broadcast_in_dim.6), calls=%async_computation.1 | async-start | bytes 8388608 | tf_op jit(solution)/shard_map/all_to_all | solution.py:493
  32.6 0.7 collective-permute-start.9
  33.3 2.9 %collective-permute-start.1 = (bf16[400,256]{1,0:T(8,128)(2,1)S(1)}, bf16[400,256]{1,0:T(8,128)(2,1)S(1)}, u32[]{:S(2)}, u32[]{:S(2)}) collective-permute-start(bf16[400,256]{1,0:T(8,128)(2,1)S(1)} %get-tuple-element.79.payload_ref), channel_id=1, source_target_pairs={{0,32},{32,64},{64,96},{96,128},{128,160},{160,192},{192,224},{224... | collective-permute-start | bytes 614408 | tf_op jit(solution)/shard_map/ppermute | solution.py:499
  36.2 0.0 collective-permute-done.9.refs_5_
  36.2 0.7 collective-permute-start.10
  36.9 6.6 %collective-permute-done.1.refs_4_ = bf16[400,256]{1,0:T(8,128)(2,1)S(1)} collective-permute-done((bf16[400,256]{1,0:T(8,128)(2,1)S(1)}, bf16[400,256]{1,0:T(8,128)(2,1)S(1)}, u32[]{:S(2)}, u32[]{:S(2)}) %collective-permute-start.1) | collective-permute-done | bytes 204832 | tf_op jit(solution)/shard_map/ppermute | solution.py:499
  43.5 1.9 %collective-permute-start.2 = (bf16[400,256]{1,0:T(8,128)(2,1)S(1)}, bf16[400,256]{1,0:T(8,128)(2,1)S(1)}, u32[]{:S(2)}, u32[]{:S(2)}) collective-permute-start(bf16[400,256]{1,0:T(8,128)(2,1)S(1)} %collective-permute-done.1.refs_4_), channel_id=1, source_target_pairs={{32,64},{64,96},{96,128},{128,160},{160,192},{192,224},{224,256},{... | collective-permute-start | bytes 614408 | tf_op jit(solution)/shard_map/ppermute | solution.py:499
  45.5 1.9 %shard_map.186 = (f32[384,128]{1,0:T(8,128)S(1)}, f32[384,128]{1,0:T(8,128)S(1)}, f32[384,128]{1,0:T(8,128)S(1)}, f32[8,256]{1,0:T(8,128)S(1)}) custom-call(s32[2]{0:T(128)S(1)} %pad_add_fusion.place_ref.refs_0_, bf16[2,384,128]{2,1,0:T(8,128)(2,1)S(1)} %get-tuple-element.76.q_ref.refs_1_, ...), custom_call_target="tpu_custom_call", output_to_operand_aliasing={{0}: (6, {}), {1}: (7, {}), {2}: (8, {}), {3}: (9, {})} | custom-call | flops 3000000000 | bytes 1000000 | tf_op jit(solution)/shard_map/pallas_call | solution.py:381
  47.4 0.0 collective-permute-done.10.refs_5_
  47.4 0.7 collective-permute-start.11
  48.1 4.9 %collective-permute-done.2.refs_4_ = bf16[400,256]{1,0:T(8,128)(2,1)S(1)} collective-permute-done((bf16[400,256]{1,0:T(8,128)(2,1)S(1)}, bf16[400,256]{1,0:T(8,128)(2,1)S(1)}, u32[]{:S(2)}, u32[]{:S(2)}) %collective-permute-start.2) | collective-permute-done | bytes 204832 | tf_op jit(solution)/shard_map/ppermute | solution.py:499
  53.0 1.9 %collective-permute-start.3 = (bf16[400,256]{1,0:T(8,128)(2,1)S(1)}, bf16[400,256]{1,0:T(8,128)(2,1)S(1)}, u32[]{:S(2)}, u32[]{:S(2)}) collective-permute-start(bf16[400,256]{1,0:T(8,128)(2,1)S(1)} %collective-permute-done.2.refs_4_), channel_id=1, source_target_pairs={{64,96},{96,128},{128,160},{160,192},{192,224},{224,256},{256,288}... | collective-permute-start | bytes 614408 | tf_op jit(solution)/shard_map/ppermute | solution.py:499
  54.9 1.9 %shard_map.187 = (f32[384,128]{1,0:T(8,128)S(1)}, f32[384,128]{1,0:T(8,128)S(1)}, f32[384,128]{1,0:T(8,128)S(1)}, f32[8,256]{1,0:T(8,128)S(1)}) custom-call(s32[2]{0:T(128)S(1)} %pad_add_fusion.place_ref.refs_0_, bf16[2,384,128]{2,1,0:T(8,128)(2,1)S(1)} %get-tuple-element.76.q_ref.refs_1_, ...), custom_call_target="tpu_custom_call", output_to_operand_aliasing={{0}: (6, {}), {1}: (7, {}), {2}: (8, {}), {3}: (9, {})} | custom-call | flops 3000000000 | bytes 1000000 | tf_op jit(solution)/shard_map/pallas_call | solution.py:381
  56.8 0.0 collective-permute-done.11.refs_5_
  56.8 1.3 collective-permute-start.12
  58.1 3.7 %collective-permute-done.3.refs_4_ = bf16[400,256]{1,0:T(8,128)(2,1)S(1)} collective-permute-done((bf16[400,256]{1,0:T(8,128)(2,1)S(1)}, bf16[400,256]{1,0:T(8,128)(2,1)S(1)}, u32[]{:S(2)}, u32[]{:S(2)}) %collective-permute-start.3) | collective-permute-done | bytes 204832 | tf_op jit(solution)/shard_map/ppermute | solution.py:499
  61.8 1.9 %collective-permute-start.4 = (bf16[400,256]{1,0:T(8,128)(2,1)S(1)}, bf16[400,256]{1,0:T(8,128)(2,1)S(1)}, u32[]{:S(2)}, u32[]{:S(2)}) collective-permute-start(bf16[400,256]{1,0:T(8,128)(2,1)S(1)} %collective-permute-done.3.refs_4_), channel_id=1, source_target_pairs={{96,128},{128,160},{160,192},{192,224},{224,256},{256,288},{288,32... | collective-permute-start | bytes 614408 | tf_op jit(solution)/shard_map/ppermute | solution.py:499
  63.7 2.1 %shard_map.188 = (f32[384,128]{1,0:T(8,128)S(1)}, f32[384,128]{1,0:T(8,128)S(1)}, f32[384,128]{1,0:T(8,128)S(1)}, f32[8,256]{1,0:T(8,128)S(1)}) custom-call(s32[2]{0:T(128)S(1)} %pad_add_fusion.place_ref.refs_0_, bf16[2,384,128]{2,1,0:T(8,128)(2,1)S(1)} %get-tuple-element.76.q_ref.refs_1_, ...), custom_call_target="tpu_custom_call", output_to_operand_aliasing={{0}: (6, {}), {1}: (7, {}), {2}: (8, {}), {3}: (9, {})} | custom-call | flops 3000000000 | bytes 1000000 | tf_op jit(solution)/shard_map/pallas_call | solution.py:381
  65.8 5.1 %collective-permute-start.13 = (bf16[400,256]{1,0:T(8,128)(2,1)S(1)}, bf16[400,256]{1,0:T(8,128)(2,1)S(1)}, u32[]{:S(2)}, u32[]{:S(2)}) collective-permute-start(bf16[400,256]{1,0:T(8,128)(2,1)S(1)} %collective-permute-done.12.refs_5_), channel_id=1, source_target_pairs={{384,352},{416,384},{448,416},{480,448},{0,480},{32,0},{64,32},{38... | collective-permute-start | bytes 614408 | tf_op jit(solution)/shard_map/ppermute | solution.py:502
  71.0 2.5 %collective-permute-start.5 = (bf16[400,256]{1,0:T(8,128)(2,1)S(1)}, bf16[400,256]{1,0:T(8,128)(2,1)S(1)}, u32[]{:S(2)}, u32[]{:S(2)}) collective-permute-start(bf16[400,256]{1,0:T(8,128)(2,1)S(1)} %collective-permute-done.4.refs_4_), channel_id=1, source_target_pairs={{128,160},{160,192},{192,224},{224,256},{256,288},{288,320},{320,3... | collective-permute-start | bytes 614408 | tf_op jit(solution)/shard_map/ppermute | solution.py:499
  73.5 3.2 %shard_map.189 = (f32[384,128]{1,0:T(8,128)S(1)}, f32[384,128]{1,0:T(8,128)S(1)}, f32[384,128]{1,0:T(8,128)S(1)}, f32[8,256]{1,0:T(8,128)S(1)}) custom-call(s32[2]{0:T(128)S(1)} %pad_add_fusion.place_ref.refs_0_, bf16[2,384,128]{2,1,0:T(8,128)(2,1)S(1)} %get-tuple-element.76.q_ref.refs_1_, ...), custom_call_target="tpu_custom_call", output_to_operand_aliasing={{0}: (6, {}), {1}: (7, {}), {2}: (8, {}), {3}: (9, {})} | custom-call | flops 3000000000 | bytes 1000000 | tf_op jit(solution)/shard_map/pallas_call | solution.py:381
  76.8 3.2 %collective-permute-start.14 = (bf16[400,256]{1,0:T(8,128)(2,1)S(1)}, bf16[400,256]{1,0:T(8,128)(2,1)S(1)}, u32[]{:S(2)}, u32[]{:S(2)}) collective-permute-start(bf16[400,256]{1,0:T(8,128)(2,1)S(1)} %collective-permute-done.13.refs_5_), channel_id=1, source_target_pairs={{352,320},{384,352},{416,384},{448,416},{480,448},{0,480},{32,0},{... | collective-permute-start | bytes 614408 | tf_op jit(solution)/shard_map/ppermute | solution.py:502
  80.0 0.0 collective-permute-done.5.refs_4_
  80.0 2.6 %collective-permute-start.6 = (bf16[400,256]{1,0:T(8,128)(2,1)S(1)}, bf16[400,256]{1,0:T(8,128)(2,1)S(1)}, u32[]{:S(2)}, u32[]{:S(2)}) collective-permute-start(bf16[400,256]{1,0:T(8,128)(2,1)S(1)} %collective-permute-done.5.refs_4_), channel_id=1, source_target_pairs={{160,192},{192,224},{224,256},{256,288},{288,320},{320,352},{352,3... | collective-permute-start | bytes 614408 | tf_op jit(solution)/shard_map/ppermute | solution.py:499
  82.6 3.2 %shard_map.190 = (f32[384,128]{1,0:T(8,128)S(1)}, f32[384,128]{1,0:T(8,128)S(1)}, f32[384,128]{1,0:T(8,128)S(1)}, f32[8,256]{1,0:T(8,128)S(1)}) custom-call(s32[2]{0:T(128)S(1)} %pad_add_fusion.place_ref.refs_0_, bf16[2,384,128]{2,1,0:T(8,128)(2,1)S(1)} %get-tuple-element.76.q_ref.refs_1_, ...), custom_call_target="tpu_custom_call", output_to_operand_aliasing={{0}: (6, {}), {1}: (7, {}), {2}: (8, {}), {3}: (9, {})} | custom-call | flops 3000000000 | bytes 1000000 | tf_op jit(solution)/shard_map/pallas_call | solution.py:381
  85.9 3.0 %collective-permute-done.6.refs_4_ = bf16[400,256]{1,0:T(8,128)(2,1)S(1)} collective-permute-done((bf16[400,256]{1,0:T(8,128)(2,1)S(1)}, bf16[400,256]{1,0:T(8,128)(2,1)S(1)}, u32[]{:S(2)}, u32[]{:S(2)}) %collective-permute-start.6) | collective-permute-done | bytes 204832 | tf_op jit(solution)/shard_map/ppermute | solution.py:499
  88.9 3.2 %shard_map.191 = (f32[384,128]{1,0:T(8,128)S(1)}, f32[384,128]{1,0:T(8,128)S(1)}, f32[384,128]{1,0:T(8,128)S(1)}, f32[8,256]{1,0:T(8,128)S(1)}) custom-call(s32[2]{0:T(128)S(1)} %pad_add_fusion.place_ref.refs_0_, bf16[2,384,128]{2,1,0:T(8,128)(2,1)S(1)} %get-tuple-element.76.q_ref.refs_1_, ...), custom_call_target="tpu_custom_call", output_to_operand_aliasing={{0}: (6, {}), {1}: (7, {}), {2}: (8, {}), {3}: (9, {})} | custom-call | flops 3000000000 | bytes 1000000 | tf_op jit(solution)/shard_map/pallas_call | solution.py:381
  92.1 1.9 %collective-permute-start.16 = (bf16[4,256,2048]{2,1,0:T(8,128)(2,1)}, bf16[4,256,2048]{2,1,0:T(8,128)(2,1)S(1)}, u32[]{:S(2)}, u32[]{:S(2)}) collective-permute-start(bf16[4,256,2048]{2,1,0:T(8,128)(2,1)} %all-to-all-done.1.mine_ref), channel_id=1, source_target_pairs={{0,1},{1,0},{2,3},{3,2},{4,5},{5,4},{6,7},{7,6},{8,9},{9,8},{10,11... | collective-permute-start | bytes 12582920 | tf_op jit(solution)/shard_map/ppermute | solution.py:515
  94.0 1.9 %collective-permute-start.7 = (bf16[400,256]{1,0:T(8,128)(2,1)S(1)}, bf16[400,256]{1,0:T(8,128)(2,1)S(1)}, u32[]{:S(2)}, u32[]{:S(2)}) collective-permute-start(bf16[400,256]{1,0:T(8,128)(2,1)S(1)} %collective-permute-done.6.refs_4_), channel_id=1, source_target_pairs={{192,224},{224,256},{256,288},{288,320},{320,352},{352,384},{384,4... | collective-permute-start | bytes 614408 | tf_op jit(solution)/shard_map/ppermute | solution.py:499
  96.0 5.1 %collective-permute-start.15 = (bf16[400,256]{1,0:T(8,128)(2,1)S(1)}, bf16[400,256]{1,0:T(8,128)(2,1)S(1)}, u32[]{:S(2)}, u32[]{:S(2)}) collective-permute-start(bf16[400,256]{1,0:T(8,128)(2,1)S(1)} %collective-permute-done.14.refs_5_), channel_id=1, source_target_pairs={{320,288},{352,320},{384,352},{416,384},{448,416},{480,448},{0,480... | collective-permute-start | bytes 614408 | tf_op jit(solution)/shard_map/ppermute | solution.py:502
  101.1 3.5 %collective-permute-done.7.refs_4_ = bf16[400,256]{1,0:T(8,128)(2,1)S(1)} collective-permute-done((bf16[400,256]{1,0:T(8,128)(2,1)S(1)}, bf16[400,256]{1,0:T(8,128)(2,1)S(1)}, u32[]{:S(2)}, u32[]{:S(2)}) %collective-permute-start.7) | collective-permute-done | bytes 204832 | tf_op jit(solution)/shard_map/ppermute | solution.py:499
  104.6 1.9 %collective-permute-start.8 = (bf16[400,256]{1,0:T(8,128)(2,1)S(1)}, bf16[400,256]{1,0:T(8,128)(2,1)S(1)}, u32[]{:S(2)}, u32[]{:S(2)}) collective-permute-start(bf16[400,256]{1,0:T(8,128)(2,1)S(1)} %collective-permute-done.7.refs_4_), channel_id=1, source_target_pairs={{224,256},{256,288},{288,320},{320,352},{352,384},{384,416},{416,4... | collective-permute-start | bytes 614408 | tf_op jit(solution)/shard_map/ppermute | solution.py:499
  106.5 3.2 %shard_map.192 = (f32[384,128]{1,0:T(8,128)S(1)}, f32[384,128]{1,0:T(8,128)S(1)}, f32[384,128]{1,0:T(8,128)S(1)}, f32[8,256]{1,0:T(8,128)S(1)}) custom-call(s32[2]{0:T(128)S(1)} %pad_add_fusion.place_ref.refs_0_, bf16[2,384,128]{2,1,0:T(8,128)(2,1)S(1)} %get-tuple-element.76.q_ref.refs_1_, ...), custom_call_target="tpu_custom_call", output_to_operand_aliasing={{0}: (6, {}), {1}: (7, {}), {2}: (8, {}), {3}: (9, {})} | custom-call | flops 3000000000 | bytes 1000000 | tf_op jit(solution)/shard_map/pallas_call | solution.py:381
  109.8 4.6 %collective-permute-done.8.refs_4_ = bf16[400,256]{1,0:T(8,128)(2,1)S(1)} collective-permute-done((bf16[400,256]{1,0:T(8,128)(2,1)S(1)}, bf16[400,256]{1,0:T(8,128)(2,1)S(1)}, u32[]{:S(2)}, u32[]{:S(2)}) %collective-permute-start.8) | collective-permute-done | bytes 204832 | tf_op jit(solution)/shard_map/ppermute | solution.py:499
  114.3 3.1 %shard_map.193 = bf16[384,256]{1,0:T(8,128)(2,1)S(1)} custom-call(s32[2]{0:T(128)S(1)} %pad_add_fusion.place_ref.refs_0_, bf16[2,384,128]{2,1,0:T(8,128)(2,1)S(1)} %get-tuple-element.76.q_ref.refs_1_, bf16[384,384]{1,0:T(8,128)(2,1)S(1)} %get-tuple-element.77.later_ref.refs_2_, f32[64,256]{1,0:T(8,128)S(1)} %get-tuple-element.78.refs_3_, ...), custom_call_target="tpu_custom_call" | custom-call | flops 3000000000 | bytes 1000000 | tf_op jit(solution)/shard_map/pallas_call | solution.py:381
  117.5 10.7 %all_to_all.15.parts_ref = bf16[8,48,256]{2,1,0:T(8,128)(2,1)S(1)} all-to-all(bf16[8,48,256]{2,1,0:T(8,128)(2,1)S(1)} %bitcast.15), channel_id=1, replica_groups=mesh['sp'=16,'fs'=4,'tp_0'=4,'tp_1'=2] {'tp_0','tp_1'}, dimensions={0} | all-to-all | bytes 393216 | tf_op jit(solution)/shard_map/all_to_all | solution.py:526
  128.2 4.7 %shard_map.194 = bf16[48,2048]{1,0:T(8,128)(2,1)} custom-call(s32[2]{0:T(128)S(1)} %pad_add_fusion.place_ref.refs_0_, bf16[8,48,256]{2,1,0:T(8,128)(2,1)S(1)} %all_to_all.15.parts_ref, bf16[4,256,2048]{2,1,0:T(8,128)(2,1)} %all-to-all-done.1.mine_ref, bf16[4,256,2048]{2,1,0:T(8,128)(2,1)S(1)} %collective-permute-done.16.other_ref), custom_call_target="tpu_custom_call" | custom-call | flops 1000000000 | bytes 10000000 | tf_op jit(solution)/shard_map/pallas_call | solution.py:528
  (15 shorter events, 0.1 us)
Async XLA Ops:
  2.0 16.6 %all-to-all-start = ((bf16[4,48,2048]{2,1,0:T(8,128)(2,1)}), bf16[4,48,2048]{2,1,0:T(8,128)(2,1)S(1)}, u32[]{:S(2)}, u32[]{:S(2)}) async-start(bf16[4,48,2048]{2,1,0:T(8,128)(2,1)} %shard_map.181), calls=%async_computation | async-start | bytes 1572864 | tf_op jit(solution)/shard_map/all_to_all | solution.py:432
  18.6 4.2 %collective-permute-start = (bf16[192,2048]{1,0:T(8,128)(2,1)S(1)}, bf16[192,2048]{1,0:T(8,128)(2,1)S(1)}, u32[]{:S(2)}, u32[]{:S(2)}) collective-permute-start(bf16[192,2048]{1,0:T(8,128)(2,1)S(1)} %bitcast.13), channel_id=1, source_target_pairs={{0,1},{1,0},{2,3},{3,2},{4,5},{5,4},{6,7},{7,6},{8,9},{9,8},{10,11... | collective-permute-start | bytes 2359304 | tf_op jit(solution)/shard_map/ppermute | solution.py:466
  21.1 3.9 %copy-start = (f32[128]{0:T(128)S(1)}, f32[128]{0:T(128)}, u32[]{:S(2)}) copy-start(f32[128]{0:T(128)} %param.35) | copy-start | bytes 1540
  27.7 64.4 %all-to-all-start.1 = ((bf16[4,256,2048]{2,1,0:T(8,128)(2,1)}), bf16[4,256,2048]{2,1,0:T(8,128)(2,1)}, u32[]{:S(2)}, u32[]{:S(2)}) async-start(bf16[4,256,2048]{2,1,0:T(8,128)(2,1)} %broadcast_in_dim.6), calls=%async_computation.1 | async-start | bytes 8388608 | tf_op jit(solution)/shard_map/all_to_all | solution.py:493
  32.6 3.6 %collective-permute-start.9 = (bf16[400,256]{1,0:T(8,128)(2,1)S(1)}, bf16[400,256]{1,0:T(8,128)(2,1)S(1)}, u32[]{:S(2)}, u32[]{:S(2)}) collective-permute-start(bf16[400,256]{1,0:T(8,128)(2,1)S(1)} %get-tuple-element.79.payload_ref), channel_id=1, source_target_pairs={{0,480},{32,0},{64,32},{96,64},{128,96},{160,128},{192,160},{1,481... | collective-permute-start | bytes 614408 | tf_op jit(solution)/shard_map/ppermute | solution.py:502
  33.3 10.2 %collective-permute-start.1 = (bf16[400,256]{1,0:T(8,128)(2,1)S(1)}, bf16[400,256]{1,0:T(8,128)(2,1)S(1)}, u32[]{:S(2)}, u32[]{:S(2)}) collective-permute-start(bf16[400,256]{1,0:T(8,128)(2,1)S(1)} %get-tuple-element.79.payload_ref), channel_id=1, source_target_pairs={{0,32},{32,64},{64,96},{96,128},{128,160},{160,192},{192,224},{224... | collective-permute-start | bytes 614408 | tf_op jit(solution)/shard_map/ppermute | solution.py:499
  36.2 11.2 %collective-permute-start.10 = (bf16[400,256]{1,0:T(8,128)(2,1)S(1)}, bf16[400,256]{1,0:T(8,128)(2,1)S(1)}, u32[]{:S(2)}, u32[]{:S(2)}) collective-permute-start(bf16[400,256]{1,0:T(8,128)(2,1)S(1)} %collective-permute-done.9.refs_5_), channel_id=1, source_target_pairs={{480,448},{0,480},{32,0},{64,32},{96,64},{128,96},{160,128},{481,4... | collective-permute-start | bytes 614408 | tf_op jit(solution)/shard_map/ppermute | solution.py:502
  43.5 9.5 %collective-permute-start.2 = (bf16[400,256]{1,0:T(8,128)(2,1)S(1)}, bf16[400,256]{1,0:T(8,128)(2,1)S(1)}, u32[]{:S(2)}, u32[]{:S(2)}) collective-permute-start(bf16[400,256]{1,0:T(8,128)(2,1)S(1)} %collective-permute-done.1.refs_4_), channel_id=1, source_target_pairs={{32,64},{64,96},{96,128},{128,160},{160,192},{192,224},{224,256},{... | collective-permute-start | bytes 614408 | tf_op jit(solution)/shard_map/ppermute | solution.py:499
  47.4 9.4 %collective-permute-start.11 = (bf16[400,256]{1,0:T(8,128)(2,1)S(1)}, bf16[400,256]{1,0:T(8,128)(2,1)S(1)}, u32[]{:S(2)}, u32[]{:S(2)}) collective-permute-start(bf16[400,256]{1,0:T(8,128)(2,1)S(1)} %collective-permute-done.10.refs_5_), channel_id=1, source_target_pairs={{448,416},{480,448},{0,480},{32,0},{64,32},{96,64},{128,96},{449,4... | collective-permute-start | bytes 614408 | tf_op jit(solution)/shard_map/ppermute | solution.py:502
  53.0 8.9 %collective-permute-start.3 = (bf16[400,256]{1,0:T(8,128)(2,1)S(1)}, bf16[400,256]{1,0:T(8,128)(2,1)S(1)}, u32[]{:S(2)}, u32[]{:S(2)}) collective-permute-start(bf16[400,256]{1,0:T(8,128)(2,1)S(1)} %collective-permute-done.2.refs_4_), channel_id=1, source_target_pairs={{64,96},{96,128},{128,160},{160,192},{192,224},{224,256},{256,288}... | collective-permute-start | bytes 614408 | tf_op jit(solution)/shard_map/ppermute | solution.py:499
  56.8 9.0 %collective-permute-start.12 = (bf16[400,256]{1,0:T(8,128)(2,1)S(1)}, bf16[400,256]{1,0:T(8,128)(2,1)S(1)}, u32[]{:S(2)}, u32[]{:S(2)}) collective-permute-start(bf16[400,256]{1,0:T(8,128)(2,1)S(1)} %collective-permute-done.11.refs_5_), channel_id=1, source_target_pairs={{416,384},{448,416},{480,448},{0,480},{32,0},{64,32},{96,64},{417,... | collective-permute-start | bytes 614408 | tf_op jit(solution)/shard_map/ppermute | solution.py:502
  61.8 9.2 %collective-permute-start.4 = (bf16[400,256]{1,0:T(8,128)(2,1)S(1)}, bf16[400,256]{1,0:T(8,128)(2,1)S(1)}, u32[]{:S(2)}, u32[]{:S(2)}) collective-permute-start(bf16[400,256]{1,0:T(8,128)(2,1)S(1)} %collective-permute-done.3.refs_4_), channel_id=1, source_target_pairs={{96,128},{128,160},{160,192},{192,224},{224,256},{256,288},{288,32... | collective-permute-start | bytes 614408 | tf_op jit(solution)/shard_map/ppermute | solution.py:499
  65.8 10.9 %collective-permute-start.13 = (bf16[400,256]{1,0:T(8,128)(2,1)S(1)}, bf16[400,256]{1,0:T(8,128)(2,1)S(1)}, u32[]{:S(2)}, u32[]{:S(2)}) collective-permute-start(bf16[400,256]{1,0:T(8,128)(2,1)S(1)} %collective-permute-done.12.refs_5_), channel_id=1, source_target_pairs={{384,352},{416,384},{448,416},{480,448},{0,480},{32,0},{64,32},{38... | collective-permute-start | bytes 614408 | tf_op jit(solution)/shard_map/ppermute | solution.py:502
  71.0 9.0 %collective-permute-start.5 = (bf16[400,256]{1,0:T(8,128)(2,1)S(1)}, bf16[400,256]{1,0:T(8,128)(2,1)S(1)}, u32[]{:S(2)}, u32[]{:S(2)}) collective-permute-start(bf16[400,256]{1,0:T(8,128)(2,1)S(1)} %collective-permute-done.4.refs_4_), channel_id=1, source_target_pairs={{128,160},{160,192},{192,224},{224,256},{256,288},{288,320},{320,3... | collective-permute-start | bytes 614408 | tf_op jit(solution)/shard_map/ppermute | solution.py:499
  76.8 9.1 %collective-permute-start.14 = (bf16[400,256]{1,0:T(8,128)(2,1)S(1)}, bf16[400,256]{1,0:T(8,128)(2,1)S(1)}, u32[]{:S(2)}, u32[]{:S(2)}) collective-permute-start(bf16[400,256]{1,0:T(8,128)(2,1)S(1)} %collective-permute-done.13.refs_5_), channel_id=1, source_target_pairs={{352,320},{384,352},{416,384},{448,416},{480,448},{0,480},{32,0},{... | collective-permute-start | bytes 614408 | tf_op jit(solution)/shard_map/ppermute | solution.py:502
  80.0 8.9 %collective-permute-start.6 = (bf16[400,256]{1,0:T(8,128)(2,1)S(1)}, bf16[400,256]{1,0:T(8,128)(2,1)S(1)}, u32[]{:S(2)}, u32[]{:S(2)}) collective-permute-start(bf16[400,256]{1,0:T(8,128)(2,1)S(1)} %collective-permute-done.5.refs_4_), channel_id=1, source_target_pairs={{160,192},{192,224},{224,256},{256,288},{288,320},{320,352},{352,3... | collective-permute-start | bytes 614408 | tf_op jit(solution)/shard_map/ppermute | solution.py:499
  92.1 36.1 %collective-permute-start.16 = (bf16[4,256,2048]{2,1,0:T(8,128)(2,1)}, bf16[4,256,2048]{2,1,0:T(8,128)(2,1)S(1)}, u32[]{:S(2)}, u32[]{:S(2)}) collective-permute-start(bf16[4,256,2048]{2,1,0:T(8,128)(2,1)} %all-to-all-done.1.mine_ref), channel_id=1, source_target_pairs={{0,1},{1,0},{2,3},{3,2},{4,5},{5,4},{6,7},{7,6},{8,9},{9,8},{10,11... | collective-permute-start | bytes 12582920 | tf_op jit(solution)/shard_map/ppermute | solution.py:515
  94.0 10.6 %collective-permute-start.7 = (bf16[400,256]{1,0:T(8,128)(2,1)S(1)}, bf16[400,256]{1,0:T(8,128)(2,1)S(1)}, u32[]{:S(2)}, u32[]{:S(2)}) collective-permute-start(bf16[400,256]{1,0:T(8,128)(2,1)S(1)} %collective-permute-done.6.refs_4_), channel_id=1, source_target_pairs={{192,224},{224,256},{256,288},{288,320},{320,352},{352,384},{384,4... | collective-permute-start | bytes 614408 | tf_op jit(solution)/shard_map/ppermute | solution.py:499
  96.0 10.6 %collective-permute-start.15 = (bf16[400,256]{1,0:T(8,128)(2,1)S(1)}, bf16[400,256]{1,0:T(8,128)(2,1)S(1)}, u32[]{:S(2)}, u32[]{:S(2)}) collective-permute-start(bf16[400,256]{1,0:T(8,128)(2,1)S(1)} %collective-permute-done.14.refs_5_), channel_id=1, source_target_pairs={{320,288},{352,320},{384,352},{416,384},{448,416},{480,448},{0,480... | collective-permute-start | bytes 614408 | tf_op jit(solution)/shard_map/ppermute | solution.py:502
  104.6 9.7 %collective-permute-start.8 = (bf16[400,256]{1,0:T(8,128)(2,1)S(1)}, bf16[400,256]{1,0:T(8,128)(2,1)S(1)}, u32[]{:S(2)}, u32[]{:S(2)}) collective-permute-start(bf16[400,256]{1,0:T(8,128)(2,1)S(1)} %collective-permute-done.7.refs_4_), channel_id=1, source_target_pairs={{224,256},{256,288},{288,320},{320,352},{352,384},{384,416},{416,4... | collective-permute-start | bytes 614408 | tf_op jit(solution)/shard_map/ppermute | solution.py:499

commit v3 on v2

--- a/solution.py
+++ b/solution.py
@@ -16,6 +16,8 @@
 F32 = jnp.float32
 BF16 = jnp.bfloat16
 
+
+PIECES = (4, 3, 5, 2)
 
 VMEM = pl.BlockSpec(memory_space=pltpu.VMEM)
 SMEM = pl.BlockSpec(memory_space=pltpu.SMEM)
@@ -80,21 +82,22 @@
     found_ref[...] = nn_dot(mine_ref[...], w_ref[...]).astype(BF16)
 
 
-def merge_kernel(place_ref, parts_ref, mine_ref, other_ref, out_ref, total_ref):
-    a = pl.program_id(0)
-    core = place_ref[1]
-
-    @pl.when(a == 0)
-    def _():
-        total_ref[...] = jnp.zeros_like(total_ref)
-
-    total_ref[...] += nn_dot(parts_ref[2 * a + core], mine_ref[0]) + nn_dot(
-        parts_ref[2 * a + 1 - core], other_ref[0]
-    )
-
-    @pl.when(a == pl.num_programs(0) - 1)
-    def _():
-        out_ref[...] = total_ref[...].astype(BF16)
+def merge_kernel(place_ref, parts_ref, *refs):
+    *weights, out_ref, held_ref, sems = refs
+    copies = [
+        pltpu.make_async_copy(ref, held_ref.at[k], sems.at[k]) for k, ref in enumerate(weights)
+    ]
+    for copy in copies:
+        copy.start()
+    core, line = place_ref[1], place_ref[2]
+    total = None
+    for k, away in enumerate(PIECES):
+        owner = (line + away) & 3
+        for j, where in ((2 * k, core), (2 * k + 1, 1 - core)):
+            copies[j].wait()
+            term = nn_dot(parts_ref[2 * owner + where], held_ref[j])
+            total = term if total is None else total + term
+    out_ref[...] = total.astype(BF16)
 
 
 def block_diagonal(parts, channels, width):
@@ -421,7 +424,7 @@
     groups = eigen_real.shape[0]
     width = groups * STATE
     channels = groups * GROUP
-    place = jnp.stack([lax.axis_index("sp"), lax.axis_index("tp_1")]).astype(jnp.int32)
+    place = jnp.stack([lax.axis_index("sp"), lax.axis_index("tp_1"), lax.axis_index("tp_0")]).astype(jnp.int32)
 
     copies = call(
         norm_kernel,
@@ -433,7 +436,6 @@
 
     w_joined = jnp.concatenate([w_input, w_query, w_key, w_value], axis=1)
     w_out = jnp.concatenate([w_out_state, w_out_attn], axis=0)
-    w_out_copies = jnp.broadcast_to(w_out[None], (4, *w_out.shape))
     decay_r, decay_i, drive_r, drive_i = discretize(
         eigen_real, eigen_imag, log_step, input_real, input_imag
     )
@@ -446,9 +448,9 @@
     bias8 = jnp.pad(jnp.transpose(key_bias).reshape(-1, 256), ((0, 5), (0, 0)))
     gains = [jnp.tile(g, 2).reshape(1, 128) for g in (query_gain, key_gain)]
     skip = skip_gain.reshape(1, -1)
-    decay, lines, reads, w_joined, w_out_copies, bias8, gains, skip, place = (
+    decay, lines, reads, w_joined, w_out, bias8, gains, skip, place = (
         lax.optimization_barrier(
-            (decay, lines, reads, w_joined, w_out_copies, bias8, gains, skip, place)
+            (decay, lines, reads, w_joined, w_out, bias8, gains, skip, place)
         )
     )
     tables = call(
@@ -489,8 +491,25 @@
         scratch=(pltpu.VMEM((rows, 2 * width), F32),),
         flops=4 * 10**9,
     )
-    acc, w_out_copies = lax.optimization_barrier((acc, w_out_copies))
-    w_out_mine = lax.all_to_all(w_out_copies, "tp_0", 0, 0, tiled=True)
+    held = {"own": w_out}
+    moves = (
+        ("left", "own", "tp_0", 1),
+        ("right", "own", "tp_0", 3),
+        ("own_swap", "own", "tp_1", 1),
+        ("far", "left", "tp_0", 1),
+        ("left_swap", "left", "tp_1", 1),
+        ("right_swap", "right", "tp_1", 1),
+        ("far_swap", "far", "tp_1", 1),
+    )
+
+    def move_weights(slot, acc):
+        name, source, axis, by = moves[slot]
+        acc, held[source] = lax.optimization_barrier((acc, held[source]))
+        size = lax.axis_size(axis)
+        held[name] = lax.ppermute(held[source], axis, [(i, (i + by) % size) for i in range(size)])
+        return acc
+
+    acc = move_weights(0, acc)
     wrap = jnp.zeros((rows, 128), F32)
     carry = jnp.zeros((8, width // 2), F32)
     up = down = payload
@@ -510,9 +529,8 @@
             flops=3 * 10**9,
             aliases={6: 0, 7: 1, 8: 2, 9: 3},
         )
-        if step == half - 2:
-            acc, w_out_mine = lax.optimization_barrier((acc, w_out_mine))
-            w_out_other = lax.ppermute(w_out_mine, "tp_1", [(0, 1), (1, 0)])
+        if step < len(moves):
+            acc = move_weights(step, acc)
     state = [shape((rows, 128)), shape((rows, 128)), shape((rows, 128)), shape(carry.shape)]
     both = call(
         lambda *refs: last_kernel(*refs, step=half, blocks=blocks, ups=half),
@@ -524,22 +542,19 @@
         flops=3 * 10**9,
     )
     parts = lax.all_to_all(both.reshape(8, piece, -1), TP, 0, 0, tiled=True)
-    columns = w_out.shape[1]
+    pieces = [held[n + end] for n in ("own", "left", "right", "far") for end in ("", "_swap")]
     return pl.pallas_call(
         merge_kernel,
-        out_shape=shape((piece, columns), BF16),
-        grid=(4,),
-        in_specs=[
-            SMEM,
-            VMEM,
-            pl.BlockSpec((1, w_out.shape[0], columns), lambda a: (a, 0, 0)),
-            pl.BlockSpec((1, w_out.shape[0], columns), lambda a: (a, 0, 0)),
+        out_shape=shape((piece, w_out.shape[1]), BF16),
+        in_specs=[SMEM, VMEM] + [pl.BlockSpec(memory_space=pl.ANY)] * len(pieces),
+        out_specs=VMEM,
+        scratch_shapes=[
+            pltpu.VMEM((len(pieces), *w_out.shape), BF16),
+            pltpu.SemaphoreType.DMA((len(pieces),)),
         ],
-        out_specs=pl.BlockSpec((piece, columns), lambda a: (0, 0)),
-        scratch_shapes=[pltpu.VMEM((piece, columns), F32)],
-        compiler_params=pltpu.CompilerParams(vmem_limit_bytes=16 * 2**20),
+        compiler_params=pltpu.CompilerParams(vmem_limit_bytes=24 * 2**20),
         cost_estimate=pl.CostEstimate(flops=10**9, bytes_accessed=10**7, transcendentals=0),
-    )(place, parts, w_out_mine, w_out_other)
+    )(place, parts, *pieces)
 
 
 def solution(mesh):

time: 134 us -> 143 us (1.067)
  the two profiles are of different devices: /device:TPU:408 before, /device:TPU:488 now
where the time goes in v3:
time: 143 us
  starting transfers between devices  60.9 us (43%)
  Pallas kernels  39.8 us (28%)
  waiting for transfers between devices  37.5 us (26%)
  other arithmetic  2.19 us (2%)
    pallas_call x13, Pallas kernels, call(): pl.pallas_call(kernel, out_shape=outs, in_specs=[SMEM] * smem + [VMEM] *...  35.6 us
    ppermute x7, starting transfers between devices, on_device(): down = lax.ppermute(down, 'sp', hops)  22.5 us
    ppermute x7, starting transfers between devices, move_weights(): lax.ppermute(held[source], axis, [(i, (i + by) % size) for i in range(siz...  17.4 us
    ppermute x8, waiting for transfers between devices, on_device(): up = lax.ppermute(up, 'sp', [(i - 1, i) for i in range(step, blocks)])  11.5 us
    ppermute x8, starting transfers between devices, on_device(): up = lax.ppermute(up, 'sp', [(i - 1, i) for i in range(step, blocks)])  10.3 us
    ppermute x7, waiting for transfers between devices, on_device(): down = lax.ppermute(down, 'sp', hops)  9.61 us
    all_to_all x1, waiting for transfers between devices, on_device(): lax.all_to_all(copies, 'tp_0', 0, 0, tiled=True).reshape(4 * piece, -1)  8.84 us
    all_to_all x1, waiting for transfers between devices, on_device(): parts = lax.all_to_all(both.reshape(8, piece, -1), TP, 0, 0, tiled=True)  6.79 us
  transfers between devices with their start and end apart: 25, of which 8 were waited for; matrix products, arithmetic and copies ran while one was open for 2% of the time, Pallas kernels for 22%

profile of v3, /device:TPU:488, one launch (start us, length us, event | category | flops | bytes accessed | tf_op | source)
XLA Modules:
  0.0 142.5 jit_solution(18044116719524645509)
XLA Ops:
  0.1 2.1 %shard_map.181 = bf16[4,48,2048]{2,1,0:T(8,128)(2,1)} custom-call(bf16[48,2048]{1,0:T(8,128)(2,1)} %tokens_ref.1, f32[1,2048]{1,0:T(1,128)} %bitcast.17), custom_call_target="tpu_custom_call" | custom-call | flops 1 | bytes 1000000 | tf_op jit(solution)/shard_map/pallas_call | solution.py:384
  2.2 4.3 %all-to-all-start = ((bf16[4,48,2048]{2,1,0:T(8,128)(2,1)}), bf16[4,48,2048]{2,1,0:T(8,128)(2,1)}, u32[]{:S(2)}, u32[]{:S(2)}) async-start(bf16[4,48,2048]{2,1,0:T(8,128)(2,1)} %shard_map.181), calls=%async_computation | async-start | bytes 1572864 | tf_op jit(solution)/shard_map/all_to_all | solution.py:435
  6.5 0.1 fusion
  6.8 0.1 reshape.32
  6.9 0.1 reshape.33
  6.9 0.1 stack_reshape.6
  7.0 0.1 stack_reshape.7
  7.1 0.1 reshape_tile.6.qg_ref
  7.2 0.1 reshape_tile.7.kg_ref
  7.3 0.1 maximum_maximum_fusion.refs_4_.refs_13_
  7.5 0.1 pad_add_fusion.place_ref.refs_0_
  7.5 0.1 pad_maximum_fusion.1.refs_0_
  7.6 1.7 %pad_maximum_fusion.w_ref = bf16[2048,512]{1,0:T(8,128)(2,1)S(1)} fusion(bf16[2048,128]{1,0:T(8,128)(2,1)} %param.24, bf16[2048,128]{1,0:T(8,128)(2,1)} %param.23, bf16[2048,128]{1,0:T(8,128)(2,1)} %param.22, bf16[2048,128]{1,0:T(8,128)(2,1)} %param.21), kind=kLoop, calls=%fused_computation | loop fusion | flops 8388608 | bytes 4194304 | tf_op jit(solution)/shard_map/concatenate | solution.py:437
  9.4 0.1 shard_map.182
  9.5 0.7 copy-done
  10.2 8.8 %all-to-all-done = bf16[4,48,2048]{2,1,0:T(8,128)(2,1)} async-done(((bf16[4,48,2048]{2,1,0:T(8,128)(2,1)}), bf16[4,48,2048]{2,1,0:T(8,128)(2,1)}, u32[]{:S(2)}, u32[]{:S(2)}) %all-to-all-start) | async-done | bytes 786464 | tf_op jit(solution)/shard_map/all_to_all | solution.py:435
  19.0 1.9 %collective-permute-start = (bf16[192,2048]{1,0:T(8,128)(2,1)}, bf16[192,2048]{1,0:T(8,128)(2,1)S(1)}, u32[]{:S(2)}, u32[]{:S(2)}) collective-permute-start(bf16[192,2048]{1,0:T(8,128)(2,1)} %bitcast.10.mine_ref), channel_id=1, source_target_pairs={{0,1},{1,0},{2,3},{3,2},{4,5},{5,4},{6,7},{7,6},{8,9},{9,8},{10,11... | collective-permute-start | bytes 2359304 | tf_op jit(solution)/shard_map/ppermute | solution.py:468
  21.0 1.7 %shard_map.183.found_ref = bf16[192,512]{1,0:T(8,128)(2,1)S(1)} custom-call(bf16[192,2048]{1,0:T(8,128)(2,1)} %bitcast.10.mine_ref, bf16[2048,512]{1,0:T(8,128)(2,1)S(1)} %pad_maximum_fusion.w_ref), custom_call_target="tpu_custom_call" | custom-call | flops 1000000000 | bytes 1000000 | tf_op jit(solution)/shard_map/pallas_call | solution.py:384
  22.7 0.0 copy-start.2
  22.7 0.7 collective-permute-done.other_ref
  23.4 2.3 %shard_map.184 = (bf16[2,384,128]{2,1,0:T(8,128)(2,1)S(1)}, bf16[400,256]{1,0:T(8,128)(2,1)S(1)}, bf16[384,128]{1,0:T(8,128)(2,1)S(1)}, f32[8,1024]{1,0:T(8,128)S(1)}) custom-call(s32[3]{0:T(128)S(1)} %pad_add_fusion.place_ref.refs_0_, bf16[192,512]{1,0:T(8,128)(2,1)S(1)} %shard_map.183.found_ref, bf16[192,2048]{1,0:T(8,128)(2,1)S(1)} %collective-permute-done.other_ref, ...), custom_call_target="tpu_custom_call" | custom-call | flops 4000000000 | bytes 1000000 | tf_op jit(solution)/shard_map/pallas_call | solution.py:384
  25.7 1.3 collective-permute-start.9
  27.0 1.3 collective-permute-start.1
  28.3 7.6 %collective-permute-done.9.refs_5_ = bf16[400,256]{1,0:T(8,128)(2,1)S(1)} collective-permute-done((bf16[400,256]{1,0:T(8,128)(2,1)S(1)}, bf16[400,256]{1,0:T(8,128)(2,1)S(1)}, u32[]{:S(2)}, u32[]{:S(2)}) %collective-permute-start.9) | collective-permute-done | bytes 204832 | tf_op jit(solution)/shard_map/ppermute | solution.py:521
  35.9 1.9 %collective-permute-start.10 = (bf16[400,256]{1,0:T(8,128)(2,1)S(1)}, bf16[400,256]{1,0:T(8,128)(2,1)S(1)}, u32[]{:S(2)}, u32[]{:S(2)}) collective-permute-start(bf16[400,256]{1,0:T(8,128)(2,1)S(1)} %collective-permute-done.9.refs_5_), channel_id=1, source_target_pairs={{480,448},{0,480},{32,0},{64,32},{96,64},{128,96},{160,128},{481,4... | collective-permute-start | bytes 614408 | tf_op jit(solution)/shard_map/ppermute | solution.py:521
  37.8 0.0 collective-permute-done.1.refs_4_
  37.8 1.3 collective-permute-start.2
  39.2 2.7 %shard_map.185 = (f32[384,128]{1,0:T(8,128)S(1)}, f32[384,128]{1,0:T(8,128)S(1)}, f32[384,128]{1,0:T(8,128)S(1)}) custom-call(bf16[2,384,128]{2,1,0:T(8,128)(2,1)S(1)} %get-tuple-element.86.q_ref.refs_1_, bf16[400,256]{1,0:T(8,128)(2,1)S(1)} %get-tuple-element.89.payload_ref, bf16[384,384]{1,0:T(8,128)(2,1)S(1)} %copy-done.1, ...), custom_call_target="tpu_custom_call" | custom-call | flops 4000000000 | bytes 1000000 | tf_op jit(solution)/shard_map/pallas_call | solution.py:384
  41.9 2.5 %collective-permute-start.16 = (bf16[256,2048]{1,0:T(8,128)(2,1)S(1)}, bf16[256,2048]{1,0:T(8,128)(2,1)S(1)}, u32[]{:S(2)}, u32[]{:S(2)}) collective-permute-start(bf16[256,2048]{1,0:T(8,128)(2,1)S(1)} %pad_maximum_fusion.1.refs_0_), channel_id=1, source_target_pairs={{0,2},{2,4},{4,6},{6,0},{1,3},{3,5},{5,7},{7,1},{8,10},{10,12},{12... | collective-permute-start | bytes 3145736 | tf_op jit(solution)/shard_map/ppermute | solution.py:509
  44.3 0.9 collective-permute-done.10.refs_5_
  45.3 3.6 %collective-permute-start.11 = (bf16[400,256]{1,0:T(8,128)(2,1)S(1)}, bf16[400,256]{1,0:T(8,128)(2,1)S(1)}, u32[]{:S(2)}, u32[]{:S(2)}) collective-permute-start(bf16[400,256]{1,0:T(8,128)(2,1)S(1)} %collective-permute-done.10.refs_5_), channel_id=1, source_target_pairs={{448,416},{480,448},{0,480},{32,0},{64,32},{96,64},{128,96},{449,4... | collective-permute-start | bytes 614408 | tf_op jit(solution)/shard_map/ppermute | solution.py:521
  48.9 0.0 collective-permute-done.2.refs_4_
  48.9 1.3 collective-permute-start.3
  50.3 3.2 %shard_map.186 = (f32[384,128]{1,0:T(8,128)S(1)}, f32[384,128]{1,0:T(8,128)S(1)}, f32[384,128]{1,0:T(8,128)S(1)}, f32[8,256]{1,0:T(8,128)S(1)}) custom-call(s32[3]{0:T(128)S(1)} %pad_add_fusion.place_ref.refs_0_, bf16[2,384,128]{2,1,0:T(8,128)(2,1)S(1)} %get-tuple-element.86.q_ref.refs_1_, ...), custom_call_target="tpu_custom_call", output_to_operand_aliasing={{0}: (6, {}), {1}: (7, {}), {2}: (8, {}), {3}: (9, {})} | custom-call | flops 3000000000 | bytes 1000000 | tf_op jit(solution)/shard_map/pallas_call | solution.py:384
  53.5 4.6 %collective-permute-start.17 = (bf16[256,2048]{1,0:T(8,128)(2,1)S(1)}, bf16[256,2048]{1,0:T(8,128)(2,1)S(1)}, u32[]{:S(2)}, u32[]{:S(2)}) collective-permute-start(bf16[256,2048]{1,0:T(8,128)(2,1)S(1)} %pad_maximum_fusion.1.refs_0_), channel_id=1, source_target_pairs={{0,6},{2,0},{4,2},{6,4},{1,7},{3,1},{5,3},{7,5},{8,14},{10,8},{12,... | collective-permute-start | bytes 3145736 | tf_op jit(solution)/shard_map/ppermute | solution.py:509
  58.1 0.0 collective-permute-done.11.refs_5_
  58.1 3.3 %collective-permute-start.12 = (bf16[400,256]{1,0:T(8,128)(2,1)S(1)}, bf16[400,256]{1,0:T(8,128)(2,1)S(1)}, u32[]{:S(2)}, u32[]{:S(2)}) collective-permute-start(bf16[400,256]{1,0:T(8,128)(2,1)S(1)} %collective-permute-done.11.refs_5_), channel_id=1, source_target_pairs={{416,384},{448,416},{480,448},{0,480},{32,0},{64,32},{96,64},{417,... | collective-permute-start | bytes 614408 | tf_op jit(solution)/shard_map/ppermute | solution.py:521
  61.4 0.0 collective-permute-done.3.refs_4_
  61.4 1.3 collective-permute-start.4
  62.7 3.2 %shard_map.187 = (f32[384,128]{1,0:T(8,128)S(1)}, f32[384,128]{1,0:T(8,128)S(1)}, f32[384,128]{1,0:T(8,128)S(1)}, f32[8,256]{1,0:T(8,128)S(1)}) custom-call(s32[3]{0:T(128)S(1)} %pad_add_fusion.place_ref.refs_0_, bf16[2,384,128]{2,1,0:T(8,128)(2,1)S(1)} %get-tuple-element.86.q_ref.refs_1_, ...), custom_call_target="tpu_custom_call", output_to_operand_aliasing={{0}: (6, {}), {1}: (7, {}), {2}: (8, {}), {3}: (9, {})} | custom-call | flops 3000000000 | bytes 1000000 | tf_op jit(solution)/shard_map/pallas_call | solution.py:384
  65.9 1.0 collective-permute-done.12.refs_5_
  67.0 3.5 %collective-permute-start.13 = (bf16[400,256]{1,0:T(8,128)(2,1)S(1)}, bf16[400,256]{1,0:T(8,128)(2,1)S(1)}, u32[]{:S(2)}, u32[]{:S(2)}) collective-permute-start(bf16[400,256]{1,0:T(8,128)(2,1)S(1)} %collective-permute-done.12.refs_5_), channel_id=1, source_target_pairs={{384,352},{416,384},{448,416},{480,448},{0,480},{32,0},{64,32},{38... | collective-permute-start | bytes 614408 | tf_op jit(solution)/shard_map/ppermute | solution.py:521
  70.5 1.3 collective-permute-start.5
  71.8 3.4 %shard_map.188 = (f32[384,128]{1,0:T(8,128)S(1)}, f32[384,128]{1,0:T(8,128)S(1)}, f32[384,128]{1,0:T(8,128)S(1)}, f32[8,256]{1,0:T(8,128)S(1)}) custom-call(s32[3]{0:T(128)S(1)} %pad_add_fusion.place_ref.refs_0_, bf16[2,384,128]{2,1,0:T(8,128)(2,1)S(1)} %get-tuple-element.86.q_ref.refs_1_, ...), custom_call_target="tpu_custom_call", output_to_operand_aliasing={{0}: (6, {}), {1}: (7, {}), {2}: (8, {}), {3}: (9, {})} | custom-call | flops 3000000000 | bytes 1000000 | tf_op jit(solution)/shard_map/pallas_call | solution.py:384
  75.2 1.9 %collective-permute-start.18 = (bf16[256,2048]{1,0:T(8,128)(2,1)S(1)}, bf16[256,2048]{1,0:T(8,128)(2,1)}, u32[]{:S(2)}, u32[]{:S(2)}) collective-permute-start(bf16[256,2048]{1,0:T(8,128)(2,1)S(1)} %collective-permute-done.16.refs_2_), channel_id=1, source_target_pairs={{0,2},{2,4},{4,6},{6,0},{1,3},{3,5},{5,7},{7,1},{8,10},{10,12},{12... | collective-permute-start | bytes 3145736 | tf_op jit(solution)/shard_map/ppermute | solution.py:509
  77.1 1.9 %collective-permute-start.19 = (bf16[256,2048]{1,0:T(8,128)(2,1)S(1)}, bf16[256,2048]{1,0:T(8,128)(2,1)}, u32[]{:S(2)}, u32[]{:S(2)}) collective-permute-start(bf16[256,2048]{1,0:T(8,128)(2,1)S(1)} %pad_maximum_fusion.1.refs_0_), channel_id=1, source_target_pairs={{0,1},{1,0},{2,3},{3,2},{4,5},{5,4},{6,7},{7,6},{8,9},{9,8},{10,11... | collective-permute-start | bytes 3145736 | tf_op jit(solution)/shard_map/ppermute | solution.py:509
  79.0 4.6 %collective-permute-start.14 = (bf16[400,256]{1,0:T(8,128)(2,1)S(1)}, bf16[400,256]{1,0:T(8,128)(2,1)S(1)}, u32[]{:S(2)}, u32[]{:S(2)}) collective-permute-start(bf16[400,256]{1,0:T(8,128)(2,1)S(1)} %collective-permute-done.13.refs_5_), channel_id=1, source_target_pairs={{352,320},{384,352},{416,384},{448,416},{480,448},{0,480},{32,0},{... | collective-permute-start | bytes 614408 | tf_op jit(solution)/shard_map/ppermute | solution.py:521
  83.6 1.3 collective-permute-start.6
  84.9 3.2 %shard_map.189 = (f32[384,128]{1,0:T(8,128)S(1)}, f32[384,128]{1,0:T(8,128)S(1)}, f32[384,128]{1,0:T(8,128)S(1)}, f32[8,256]{1,0:T(8,128)S(1)}) custom-call(s32[3]{0:T(128)S(1)} %pad_add_fusion.place_ref.refs_0_, bf16[2,384,128]{2,1,0:T(8,128)(2,1)S(1)} %get-tuple-element.86.q_ref.refs_1_, ...), custom_call_target="tpu_custom_call", output_to_operand_aliasing={{0}: (6, {}), {1}: (7, {}), {2}: (8, {}), {3}: (9, {})} | custom-call | flops 3000000000 | bytes 1000000 | tf_op jit(solution)/shard_map/pallas_call | solution.py:384
  88.2 3.2 %shard_map.190 = (f32[384,128]{1,0:T(8,128)S(1)}, f32[384,128]{1,0:T(8,128)S(1)}, f32[384,128]{1,0:T(8,128)S(1)}, f32[8,256]{1,0:T(8,128)S(1)}) custom-call(s32[3]{0:T(128)S(1)} %pad_add_fusion.place_ref.refs_0_, bf16[2,384,128]{2,1,0:T(8,128)(2,1)S(1)} %get-tuple-element.86.q_ref.refs_1_, ...), custom_call_target="tpu_custom_call", output_to_operand_aliasing={{0}: (6, {}), {1}: (7, {}), {2}: (8, {}), {3}: (9, {})} | custom-call | flops 3000000000 | bytes 1000000 | tf_op jit(solution)/shard_map/pallas_call | solution.py:384
  91.4 2.1 %collective-permute-start.20 = (bf16[256,2048]{1,0:T(8,128)(2,1)S(1)}, bf16[256,2048]{1,0:T(8,128)(2,1)}, u32[]{:S(2)}, u32[]{:S(2)}) collective-permute-start(bf16[256,2048]{1,0:T(8,128)(2,1)S(1)} %collective-permute-done.16.refs_2_), channel_id=1, source_target_pairs={{0,1},{1,0},{2,3},{3,2},{4,5},{5,4},{6,7},{7,6},{8,9},{9,8},{10,11... | collective-permute-start | bytes 3145736 | tf_op jit(solution)/shard_map/ppermute | solution.py:509
  93.6 4.3 %collective-permute-start.15 = (bf16[400,256]{1,0:T(8,128)(2,1)S(1)}, bf16[400,256]{1,0:T(8,128)(2,1)S(1)}, u32[]{:S(2)}, u32[]{:S(2)}) collective-permute-start(bf16[400,256]{1,0:T(8,128)(2,1)S(1)} %collective-permute-done.14.refs_5_), channel_id=1, source_target_pairs={{320,288},{352,320},{384,352},{416,384},{448,416},{480,448},{0,480... | collective-permute-start | bytes 614408 | tf_op jit(solution)/shard_map/ppermute | solution.py:521
  97.9 2.1 %collective-permute-start.21 = (bf16[256,2048]{1,0:T(8,128)(2,1)S(1)}, bf16[256,2048]{1,0:T(8,128)(2,1)}, u32[]{:S(2)}, u32[]{:S(2)}) collective-permute-start(bf16[256,2048]{1,0:T(8,128)(2,1)S(1)} %collective-permute-done.17.refs_4_), channel_id=1, source_target_pairs={{0,1},{1,0},{2,3},{3,2},{4,5},{5,4},{6,7},{7,6},{8,9},{9,8},{10,11... | collective-permute-start | bytes 3145736 | tf_op jit(solution)/shard_map/ppermute | solution.py:509
  100.0 3.2 %shard_map.191 = (f32[384,128]{1,0:T(8,128)S(1)}, f32[384,128]{1,0:T(8,128)S(1)}, f32[384,128]{1,0:T(8,128)S(1)}, f32[8,256]{1,0:T(8,128)S(1)}) custom-call(s32[3]{0:T(128)S(1)} %pad_add_fusion.place_ref.refs_0_, bf16[2,384,128]{2,1,0:T(8,128)(2,1)S(1)} %get-tuple-element.86.q_ref.refs_1_, ...), custom_call_target="tpu_custom_call", output_to_operand_aliasing={{0}: (6, {}), {1}: (7, {}), {2}: (8, {}), {3}: (9, {})} | custom-call | flops 3000000000 | bytes 1000000 | tf_op jit(solution)/shard_map/pallas_call | solution.py:384
  103.3 2.2 %collective-permute-start.22 = (bf16[256,2048]{1,0:T(8,128)(2,1)}, bf16[256,2048]{1,0:T(8,128)(2,1)}, u32[]{:S(2)}, u32[]{:S(2)}) collective-permute-start(bf16[256,2048]{1,0:T(8,128)(2,1)} %collective-permute-done.18.refs_6_), channel_id=1, source_target_pairs={{0,1},{1,0},{2,3},{3,2},{4,5},{5,4},{6,7},{7,6},{8,9},{9,8},{10,11... | collective-permute-start | bytes 3145736 | tf_op jit(solution)/shard_map/ppermute | solution.py:509
  105.5 1.3 collective-permute-start.7
  106.8 7.8 %collective-permute-done.7.refs_4_ = bf16[400,256]{1,0:T(8,128)(2,1)S(1)} collective-permute-done((bf16[400,256]{1,0:T(8,128)(2,1)S(1)}, bf16[400,256]{1,0:T(8,128)(2,1)S(1)}, u32[]{:S(2)}, u32[]{:S(2)}) %collective-permute-start.7) | collective-permute-done | bytes 204832 | tf_op jit(solution)/shard_map/ppermute | solution.py:518
  114.6 1.3 collective-permute-start.8
  115.9 3.2 %shard_map.192 = (f32[384,128]{1,0:T(8,128)S(1)}, f32[384,128]{1,0:T(8,128)S(1)}, f32[384,128]{1,0:T(8,128)S(1)}, f32[8,256]{1,0:T(8,128)S(1)}) custom-call(s32[3]{0:T(128)S(1)} %pad_add_fusion.place_ref.refs_0_, bf16[2,384,128]{2,1,0:T(8,128)(2,1)S(1)} %get-tuple-element.86.q_ref.refs_1_, ...), custom_call_target="tpu_custom_call", output_to_operand_aliasing={{0}: (6, {}), {1}: (7, {}), {2}: (8, {}), {3}: (9, {})} | custom-call | flops 3000000000 | bytes 1000000 | tf_op jit(solution)/shard_map/pallas_call | solution.py:384
  119.1 3.7 %collective-permute-done.8.refs_4_ = bf16[400,256]{1,0:T(8,128)(2,1)S(1)} collective-permute-done((bf16[400,256]{1,0:T(8,128)(2,1)S(1)}, bf16[400,256]{1,0:T(8,128)(2,1)S(1)}, u32[]{:S(2)}, u32[]{:S(2)}) %collective-permute-start.8) | collective-permute-done | bytes 204832 | tf_op jit(solution)/shard_map/ppermute | solution.py:518
  122.8 4.0 %shard_map.193 = bf16[384,256]{1,0:T(8,128)(2,1)} custom-call(s32[3]{0:T(128)S(1)} %pad_add_fusion.place_ref.refs_0_, bf16[2,384,128]{2,1,0:T(8,128)(2,1)S(1)} %get-tuple-element.86.q_ref.refs_1_, bf16[384,384]{1,0:T(8,128)(2,1)S(1)} %copy-done.1, f32[64,256]{1,0:T(8,128)S(1)} %get-tuple-element.88.refs_3_, ...), custom_call_target="tpu_custom_call" | custom-call | flops 3000000000 | bytes 1000000 | tf_op jit(solution)/shard_map/pallas_call | solution.py:384
  126.8 4.5 %all-to-all-start.1 = ((bf16[8,48,256]{2,1,0:T(8,128)(2,1)}), bf16[8,48,256]{2,1,0:T(8,128)(2,1)S(1)}, u32[]{:S(2)}, u32[]{:S(2)}) async-start(bf16[8,48,256]{2,1,0:T(8,128)(2,1)} %bitcast.11), calls=%async_computation.1 | async-start | bytes 393216 | tf_op jit(solution)/shard_map/all_to_all | solution.py:544
  131.3 6.8 %all-to-all-done.1.parts_ref = bf16[8,48,256]{2,1,0:T(8,128)(2,1)S(1)} async-done(((bf16[8,48,256]{2,1,0:T(8,128)(2,1)}), bf16[8,48,256]{2,1,0:T(8,128)(2,1)S(1)}, u32[]{:S(2)}, u32[]{:S(2)}) %all-to-all-start.1) | async-done | bytes 196640 | tf_op jit(solution)/shard_map/all_to_all | solution.py:544
  138.1 4.2 %shard_map.194 = bf16[48,2048]{1,0:T(8,128)(2,1)} custom-call(s32[3]{0:T(128)S(1)} %pad_add_fusion.place_ref.refs_0_, bf16[8,48,256]{2,1,0:T(8,128)(2,1)S(1)} %all-to-all-done.1.parts_ref, bf16[256,2048]{1,0:T(8,128)(2,1)S(1)} %pad_maximum_fusion.1.refs_0_, bf16[256,2048]{1,0:T(8,128)(2,1)} %collective-permute-done.19.refs_1_, ...), custom_call_target="tpu_custom_call" | custom-call | flops 1000000000 | bytes 10000000 | tf_op jit(solution)/shard_map/pallas_call | solution.py:546
  (53 shorter events, 0.2 us)
Async XLA Ops:
  0.0 6.5 %copy-start.12 = (f32[8]{0:T(128)S(1)}, f32[8]{0:T(128)}, u32[]{:S(2)}) copy-start(f32[8]{0:T(128)} %param.30) | copy-start | bytes 100
  0.0 6.5 %copy-start.10 = (f32[8,64]{1,0:T(8,128)S(1)}, f32[8,64]{1,0:T(8,128)}, u32[]{:S(2)}) copy-start(f32[8,64]{1,0:T(8,128)} %param.28) | copy-start | bytes 6148
  0.0 6.5 %copy-start.9 = (f32[8,64]{1,0:T(8,128)S(1)}, f32[8,64]{1,0:T(8,128)}, u32[]{:S(2)}) copy-start(f32[8,64]{1,0:T(8,128)} %param.29) | copy-start | bytes 6148
  0.0 6.7 %copy-start.6 = (f32[8,64,16]{1,2,0:T(8,128)S(1)}, f32[8,64,16]{1,2,0:T(8,128)}, u32[]{:S(2)}) copy-start(f32[8,64,16]{1,2,0:T(8,128)} %param.31) | copy-start | bytes 98308
  0.0 6.7 %copy-start.5 = (f32[8,64,16]{1,2,0:T(8,128)S(1)}, f32[8,64,16]{1,2,0:T(8,128)}, u32[]{:S(2)}) copy-start(f32[8,64,16]{1,2,0:T(8,128)} %param.32) | copy-start | bytes 98308
  0.0 7.1 %copy-start.11 = (bf16[384,2]{0,1:T(2,128)(2,1)S(1)}, bf16[384,2]{0,1:T(2,128)(2,1)}, u32[]{:S(2)}) copy-start(bf16[384,2]{0,1:T(2,128)(2,1)} %param.27) | copy-start | bytes 4612
  0.0 7.1 %copy-start.13 = (f32[64]{0:T(128)S(1)}, f32[64]{0:T(128)}, u32[]{:S(2)}) copy-start(f32[64]{0:T(128)} %param.25) | copy-start | bytes 772
  0.0 7.2 %copy-start.14 = (f32[64]{0:T(128)S(1)}, f32[64]{0:T(128)}, u32[]{:S(2)}) copy-start(f32[64]{0:T(128)} %param.26) | copy-start | bytes 772
  0.1 7.3 %copy-start.8 = (f32[8,16,64]{2,1,0:T(8,128)S(1)}, f32[8,16,64]{2,1,0:T(8,128)}, u32[]{:S(2)}) copy-start(f32[8,16,64]{2,1,0:T(8,128)} %param.33) | copy-start | bytes 98308
  0.1 7.3 %copy-start.7 = (f32[8,16,64]{2,1,0:T(8,128)S(1)}, f32[8,16,64]{2,1,0:T(8,128)}, u32[]{:S(2)}) copy-start(f32[8,16,64]{2,1,0:T(8,128)} %param.34) | copy-start | bytes 98308
  0.1 7.5 %copy-start.4 = (bf16[128,2048]{1,0:T(8,128)(2,1)S(1)}, bf16[128,2048]{1,0:T(8,128)(2,1)}, u32[]{:S(2)}) copy-start(bf16[128,2048]{1,0:T(8,128)(2,1)} %param.36) | copy-start | bytes 1572868
  0.1 7.4 %copy-start.3 = (bf16[128,2048]{1,0:T(8,128)(2,1)S(1)}, bf16[128,2048]{1,0:T(8,128)(2,1)}, u32[]{:S(2)}) copy-start(bf16[128,2048]{1,0:T(8,128)(2,1)} %param.37) | copy-start | bytes 1572868
  2.2 16.8 %all-to-all-start = ((bf16[4,48,2048]{2,1,0:T(8,128)(2,1)}), bf16[4,48,2048]{2,1,0:T(8,128)(2,1)}, u32[]{:S(2)}, u32[]{:S(2)}) async-start(bf16[4,48,2048]{2,1,0:T(8,128)(2,1)} %shard_map.181), calls=%async_computation | async-start | bytes 1572864 | tf_op jit(solution)/shard_map/all_to_all | solution.py:435
  9.5 0.7 copy-start
  19.0 4.4 %collective-permute-start = (bf16[192,2048]{1,0:T(8,128)(2,1)}, bf16[192,2048]{1,0:T(8,128)(2,1)S(1)}, u32[]{:S(2)}, u32[]{:S(2)}) collective-permute-start(bf16[192,2048]{1,0:T(8,128)(2,1)} %bitcast.10.mine_ref), channel_id=1, source_target_pairs={{0,1},{1,0},{2,3},{3,2},{4,5},{5,4},{6,7},{7,6},{8,9},{9,8},{10,11... | collective-permute-start | bytes 2359304 | tf_op jit(solution)/shard_map/ppermute | solution.py:468
  22.7 16.5 %copy-start.1 = (bf16[384,384]{1,0:T(8,128)(2,1)S(1)}, bf16[384,384]{1,0:T(8,128)(2,1)}, u32[]{:S(2)}) copy-start(bf16[384,384]{1,0:T(8,128)(2,1)} %copy-done) | copy-start | bytes 884740
  22.7 16.5 %copy-start.2 = (f32[128]{0:T(128)S(1)}, f32[128]{0:T(128)}, u32[]{:S(2)}) copy-start(f32[128]{0:T(128)} %param.35) | copy-start | bytes 1540
  25.7 10.2 %collective-permute-start.9 = (bf16[400,256]{1,0:T(8,128)(2,1)S(1)}, bf16[400,256]{1,0:T(8,128)(2,1)S(1)}, u32[]{:S(2)}, u32[]{:S(2)}) collective-permute-start(bf16[400,256]{1,0:T(8,128)(2,1)S(1)} %get-tuple-element.89.payload_ref), channel_id=1, source_target_pairs={{0,480},{32,0},{64,32},{96,64},{128,96},{160,128},{192,160},{1,481... | collective-permute-start | bytes 614408 | tf_op jit(solution)/shard_map/ppermute | solution.py:521
  27.0 10.8 %collective-permute-start.1 = (bf16[400,256]{1,0:T(8,128)(2,1)S(1)}, bf16[400,256]{1,0:T(8,128)(2,1)S(1)}, u32[]{:S(2)}, u32[]{:S(2)}) collective-permute-start(bf16[400,256]{1,0:T(8,128)(2,1)S(1)} %get-tuple-element.89.payload_ref), channel_id=1, source_target_pairs={{0,32},{32,64},{64,96},{96,128},{128,160},{160,192},{192,224},{224... | collective-permute-start | bytes 614408 | tf_op jit(solution)/shard_map/ppermute | solution.py:518
  35.9 9.4 %collective-permute-start.10 = (bf16[400,256]{1,0:T(8,128)(2,1)S(1)}, bf16[400,256]{1,0:T(8,128)(2,1)S(1)}, u32[]{:S(2)}, u32[]{:S(2)}) collective-permute-start(bf16[400,256]{1,0:T(8,128)(2,1)S(1)} %collective-permute-done.9.refs_5_), channel_id=1, source_target_pairs={{480,448},{0,480},{32,0},{64,32},{96,64},{128,96},{160,128},{481,4... | collective-permute-start | bytes 614408 | tf_op jit(solution)/shard_map/ppermute | solution.py:521
  37.8 11.1 %collective-permute-start.2 = (bf16[400,256]{1,0:T(8,128)(2,1)S(1)}, bf16[400,256]{1,0:T(8,128)(2,1)S(1)}, u32[]{:S(2)}, u32[]{:S(2)}) collective-permute-start(bf16[400,256]{1,0:T(8,128)(2,1)S(1)} %collective-permute-done.1.refs_4_), channel_id=1, source_target_pairs={{32,64},{64,96},{96,128},{128,160},{160,192},{192,224},{224,256},{... | collective-permute-start | bytes 614408 | tf_op jit(solution)/shard_map/ppermute | solution.py:518
  41.9 33.3 %collective-permute-start.16 = (bf16[256,2048]{1,0:T(8,128)(2,1)S(1)}, bf16[256,2048]{1,0:T(8,128)(2,1)S(1)}, u32[]{:S(2)}, u32[]{:S(2)}) collective-permute-start(bf16[256,2048]{1,0:T(8,128)(2,1)S(1)} %pad_maximum_fusion.1.refs_0_), channel_id=1, source_target_pairs={{0,2},{2,4},{4,6},{6,0},{1,3},{3,5},{5,7},{7,1},{8,10},{10,12},{12... | collective-permute-start | bytes 3145736 | tf_op jit(solution)/shard_map/ppermute | solution.py:509
  45.3 12.8 %collective-permute-start.11 = (bf16[400,256]{1,0:T(8,128)(2,1)S(1)}, bf16[400,256]{1,0:T(8,128)(2,1)S(1)}, u32[]{:S(2)}, u32[]{:S(2)}) collective-permute-start(bf16[400,256]{1,0:T(8,128)(2,1)S(1)} %collective-permute-done.10.refs_5_), channel_id=1, source_target_pairs={{448,416},{480,448},{0,480},{32,0},{64,32},{96,64},{128,96},{449,4... | collective-permute-start | bytes 614408 | tf_op jit(solution)/shard_map/ppermute | solution.py:521
  48.9 12.4 %collective-permute-start.3 = (bf16[400,256]{1,0:T(8,128)(2,1)S(1)}, bf16[400,256]{1,0:T(8,128)(2,1)S(1)}, u32[]{:S(2)}, u32[]{:S(2)}) collective-permute-start(bf16[400,256]{1,0:T(8,128)(2,1)S(1)} %collective-permute-done.2.refs_4_), channel_id=1, source_target_pairs={{64,96},{96,128},{128,160},{160,192},{192,224},{224,256},{256,288}... | collective-permute-start | bytes 614408 | tf_op jit(solution)/shard_map/ppermute | solution.py:518
  53.5 40.1 %collective-permute-start.17 = (bf16[256,2048]{1,0:T(8,128)(2,1)S(1)}, bf16[256,2048]{1,0:T(8,128)(2,1)S(1)}, u32[]{:S(2)}, u32[]{:S(2)}) collective-permute-start(bf16[256,2048]{1,0:T(8,128)(2,1)S(1)} %pad_maximum_fusion.1.refs_0_), channel_id=1, source_target_pairs={{0,6},{2,0},{4,2},{6,4},{1,7},{3,1},{5,3},{7,5},{8,14},{10,8},{12,... | collective-permute-start | bytes 3145736 | tf_op jit(solution)/shard_map/ppermute | solution.py:509
  58.1 8.9 %collective-permute-start.12 = (bf16[400,256]{1,0:T(8,128)(2,1)S(1)}, bf16[400,256]{1,0:T(8,128)(2,1)S(1)}, u32[]{:S(2)}, u32[]{:S(2)}) collective-permute-start(bf16[400,256]{1,0:T(8,128)(2,1)S(1)} %collective-permute-done.11.refs_5_), channel_id=1, source_target_pairs={{416,384},{448,416},{480,448},{0,480},{32,0},{64,32},{96,64},{417,... | collective-permute-start | bytes 614408 | tf_op jit(solution)/shard_map/ppermute | solution.py:521
  61.4 9.1 %collective-permute-start.4 = (bf16[400,256]{1,0:T(8,128)(2,1)S(1)}, bf16[400,256]{1,0:T(8,128)(2,1)S(1)}, u32[]{:S(2)}, u32[]{:S(2)}) collective-permute-start(bf16[400,256]{1,0:T(8,128)(2,1)S(1)} %collective-permute-done.3.refs_4_), channel_id=1, source_target_pairs={{96,128},{128,160},{160,192},{192,224},{224,256},{256,288},{288,32... | collective-permute-start | bytes 614408 | tf_op jit(solution)/shard_map/ppermute | solution.py:518
  67.0 12.1 %collective-permute-start.13 = (bf16[400,256]{1,0:T(8,128)(2,1)S(1)}, bf16[400,256]{1,0:T(8,128)(2,1)S(1)}, u32[]{:S(2)}, u32[]{:S(2)}) collective-permute-start(bf16[400,256]{1,0:T(8,128)(2,1)S(1)} %collective-permute-done.12.refs_5_), channel_id=1, source_target_pairs={{384,352},{416,384},{448,416},{480,448},{0,480},{32,0},{64,32},{38... | collective-permute-start | bytes 614408 | tf_op jit(solution)/shard_map/ppermute | solution.py:521
  70.5 13.2 %collective-permute-start.5 = (bf16[400,256]{1,0:T(8,128)(2,1)S(1)}, bf16[400,256]{1,0:T(8,128)(2,1)S(1)}, u32[]{:S(2)}, u32[]{:S(2)}) collective-permute-start(bf16[400,256]{1,0:T(8,128)(2,1)S(1)} %collective-permute-done.4.refs_4_), channel_id=1, source_target_pairs={{128,160},{160,192},{192,224},{224,256},{256,288},{288,320},{320,3... | collective-permute-start | bytes 614408 | tf_op jit(solution)/shard_map/ppermute | solution.py:518
  75.2 28.1 %collective-permute-start.18 = (bf16[256,2048]{1,0:T(8,128)(2,1)S(1)}, bf16[256,2048]{1,0:T(8,128)(2,1)}, u32[]{:S(2)}, u32[]{:S(2)}) collective-permute-start(bf16[256,2048]{1,0:T(8,128)(2,1)S(1)} %collective-permute-done.16.refs_2_), channel_id=1, source_target_pairs={{0,2},{2,4},{4,6},{6,0},{1,3},{3,5},{5,7},{7,1},{8,10},{10,12},{12... | collective-permute-start | bytes 3145736 | tf_op jit(solution)/shard_map/ppermute | solution.py:509
  77.1 54.2 %collective-permute-start.19 = (bf16[256,2048]{1,0:T(8,128)(2,1)S(1)}, bf16[256,2048]{1,0:T(8,128)(2,1)}, u32[]{:S(2)}, u32[]{:S(2)}) collective-permute-start(bf16[256,2048]{1,0:T(8,128)(2,1)S(1)} %pad_maximum_fusion.1.refs_0_), channel_id=1, source_target_pairs={{0,1},{1,0},{2,3},{3,2},{4,5},{5,4},{6,7},{7,6},{8,9},{9,8},{10,11... | collective-permute-start | bytes 3145736 | tf_op jit(solution)/shard_map/ppermute | solution.py:509
  79.0 12.4 %collective-permute-start.14 = (bf16[400,256]{1,0:T(8,128)(2,1)S(1)}, bf16[400,256]{1,0:T(8,128)(2,1)S(1)}, u32[]{:S(2)}, u32[]{:S(2)}) collective-permute-start(bf16[400,256]{1,0:T(8,128)(2,1)S(1)} %collective-permute-done.13.refs_5_), channel_id=1, source_target_pairs={{352,320},{384,352},{416,384},{448,416},{480,448},{0,480},{32,0},{... | collective-permute-start | bytes 614408 | tf_op jit(solution)/shard_map/ppermute | solution.py:521
  83.6 14.2 %collective-permute-start.6 = (bf16[400,256]{1,0:T(8,128)(2,1)S(1)}, bf16[400,256]{1,0:T(8,128)(2,1)S(1)}, u32[]{:S(2)}, u32[]{:S(2)}) collective-permute-start(bf16[400,256]{1,0:T(8,128)(2,1)S(1)} %collective-permute-done.5.refs_4_), channel_id=1, source_target_pairs={{160,192},{192,224},{224,256},{256,288},{288,320},{320,352},{352,3... | collective-permute-start | bytes 614408 | tf_op jit(solution)/shard_map/ppermute | solution.py:518
  91.4 39.9 %collective-permute-start.20 = (bf16[256,2048]{1,0:T(8,128)(2,1)S(1)}, bf16[256,2048]{1,0:T(8,128)(2,1)}, u32[]{:S(2)}, u32[]{:S(2)}) collective-permute-start(bf16[256,2048]{1,0:T(8,128)(2,1)S(1)} %collective-permute-done.16.refs_2_), channel_id=1, source_target_pairs={{0,1},{1,0},{2,3},{3,2},{4,5},{5,4},{6,7},{7,6},{8,9},{9,8},{10,11... | collective-permute-start | bytes 3145736 | tf_op jit(solution)/shard_map/ppermute | solution.py:509
  93.6 11.9 %collective-permute-start.15 = (bf16[400,256]{1,0:T(8,128)(2,1)S(1)}, bf16[400,256]{1,0:T(8,128)(2,1)S(1)}, u32[]{:S(2)}, u32[]{:S(2)}) collective-permute-start(bf16[400,256]{1,0:T(8,128)(2,1)S(1)} %collective-permute-done.14.refs_5_), channel_id=1, source_target_pairs={{320,288},{352,320},{384,352},{416,384},{448,416},{480,448},{0,480... | collective-permute-start | bytes 614408 | tf_op jit(solution)/shard_map/ppermute | solution.py:521
  97.9 40.2 %collective-permute-start.21 = (bf16[256,2048]{1,0:T(8,128)(2,1)S(1)}, bf16[256,2048]{1,0:T(8,128)(2,1)}, u32[]{:S(2)}, u32[]{:S(2)}) collective-permute-start(bf16[256,2048]{1,0:T(8,128)(2,1)S(1)} %collective-permute-done.17.refs_4_), channel_id=1, source_target_pairs={{0,1},{1,0},{2,3},{3,2},{4,5},{5,4},{6,7},{7,6},{8,9},{9,8},{10,11... | collective-permute-start | bytes 3145736 | tf_op jit(solution)/shard_map/ppermute | solution.py:509
  103.3 34.8 %collective-permute-start.22 = (bf16[256,2048]{1,0:T(8,128)(2,1)}, bf16[256,2048]{1,0:T(8,128)(2,1)}, u32[]{:S(2)}, u32[]{:S(2)}) collective-permute-start(bf16[256,2048]{1,0:T(8,128)(2,1)} %collective-permute-done.18.refs_6_), channel_id=1, source_target_pairs={{0,1},{1,0},{2,3},{3,2},{4,5},{5,4},{6,7},{7,6},{8,9},{9,8},{10,11... | collective-permute-start | bytes 3145736 | tf_op jit(solution)/shard_map/ppermute | solution.py:509
  105.5 9.1 %collective-permute-start.7 = (bf16[400,256]{1,0:T(8,128)(2,1)S(1)}, bf16[400,256]{1,0:T(8,128)(2,1)S(1)}, u32[]{:S(2)}, u32[]{:S(2)}) collective-permute-start(bf16[400,256]{1,0:T(8,128)(2,1)S(1)} %collective-permute-done.6.refs_4_), channel_id=1, source_target_pairs={{192,224},{224,256},{256,288},{288,320},{320,352},{352,384},{384,4... | collective-permute-start | bytes 614408 | tf_op jit(solution)/shard_map/ppermute | solution.py:518
  114.6 8.2 %collective-permute-start.8 = (bf16[400,256]{1,0:T(8,128)(2,1)S(1)}, bf16[400,256]{1,0:T(8,128)(2,1)S(1)}, u32[]{:S(2)}, u32[]{:S(2)}) collective-permute-start(bf16[400,256]{1,0:T(8,128)(2,1)S(1)} %collective-permute-done.7.refs_4_), channel_id=1, source_target_pairs={{224,256},{256,288},{288,320},{320,352},{352,384},{384,416},{416,4... | collective-permute-start | bytes 614408 | tf_op jit(solution)/shard_map/ppermute | solution.py:518
  126.8 11.3 %all-to-all-start.1 = ((bf16[8,48,256]{2,1,0:T(8,128)(2,1)}), bf16[8,48,256]{2,1,0:T(8,128)(2,1)S(1)}, u32[]{:S(2)}, u32[]{:S(2)}) async-start(bf16[8,48,256]{2,1,0:T(8,128)(2,1)} %bitcast.11), calls=%async_computation.1 | async-start | bytes 393216 | tf_op jit(solution)/shard_map/all_to_all | solution.py:544
